TPU v7x, 256 devices: a 4x2x16 block of a 4x16x16 slice. The times are simulated.
256 devices in a mesh: grp: 2 (over y), sp: 32 (over z, core), tp: 4 (over x).
Axes of the slice: x: 4, y: 2, z: 16, core: 2. Of those that a mesh axis runs over, the one named last changes fastest.
The devices are a block of a 4x16x16 slice.
Arguments:
- residual: bfloat16 [16384, 3072], P(('grp', 'sp', 'tp')), parts along dimension 0, may hold values from -3 to 3
- query_latent: bfloat16 [16384, 768], P(('grp', 'sp')), parts along dimension 0, may hold values from -6 to 6
- kv_latent: bfloat16 [16384, 384], P(('grp', 'sp')), parts along dimension 0, may hold values from -6 to 6
- rotary_key: bfloat16 [16384, 64], P(('grp', 'sp')), parts along dimension 0, may hold values from -384 to 384
- doc_ids: int32 [16384], P(('grp', 'sp')), parts along dimension 0, may hold values from 0 to 3, never falling along the last dimension, each value on 1 to 4352 neighbouring positions
- query_gain: float32 [768], replicated, may hold values from 0.1 to 1.9
- kv_gain: float32 [384], replicated, may hold values from 0.1 to 1.9
- w_query_nope: bfloat16 [768, 1536], P(None, 'tp'), may hold values from -0.625 to 0.625
- w_query_rot: bfloat16 [768, 768], P(None, 'tp'), may hold values from -0.625 to 0.625
- w_key_nope: bfloat16 [384, 1536], P(None, 'tp'), may hold values from -0.3125 to 0.3125
- w_value: bfloat16 [384, 1536], P(None, 'tp'), may hold values from -0.3125 to 0.3125
- w_out: bfloat16 [1536, 3072], P('tp'), may hold values from -0.3125 to 0.3125
- ffn_gain: float32 [3072], replicated, may hold values from 0.1 to 1.9
- w_gate: bfloat16 [32, 3072, 768], P('sp', None, 'tp'), may hold values from -0.109375 to 0.109375
- w_up: bfloat16 [32, 3072, 768], P('sp', None, 'tp'), may hold values from -0.109375 to 0.109375
- w_down: bfloat16 [32, 768, 3072], P('sp', 'tp'), may hold values from -0.4375 to 0.4375
- routes: int32 [16384, 2], P(('grp', 'sp', 'tp')), parts along dimension 0, may hold values from 0 to 31, as said below
- group_weight: float32 [16384], P(('grp', 'sp', 'tp')), parts along dimension 0, may hold values from 0.2 to 1
- member_logits: float32 [16384, 2], P(('grp', 'sp', 'tp')), parts along dimension 0, may hold values from -6 to 406
Outputs:
- layer_out: bfloat16 [16384, 3072], P(('grp', 'sp', 'tp')), parts along dimension 0
There are 2 independent parts, one for each index of `grp`. A program takes and returns all parts, laid end to end along the dimension named above; an argument that names none is the same for every part. Nothing has to cross between parts.
Inputs may be any that keep to these rules, and one draw needn't show every extreme that they name: `routes`: the two experts of a token differ and lie in one group of 8 experts (expert e belongs to group e // 8). The 64 tokens of one device, in aligned blocks, send exactly 4 assignments to each expert. `doc_ids`: document numbers never fall along the sequence; each document has 1 to 4352 positions, one exactly 4352.
All inputs are finite; a program needn't handle non-finite values.
Results may differ from a plain program's by a relative error of at most 0.019.
The roundings to bfloat16 on the way count: a program that leaves them out, or rounds other values in their place, can miss the bound.
Values may be sent and summed in bfloat16 or wider, within the bound.
A program may use at most 128 MiB of HBM per device.

v0:
```python
import jax
import jax.numpy as jnp
from jax import lax
from jax.sharding import PartitionSpec as P

NOPE = 128
ROPE = 64
VDIM = 128


EPSILON = 1e-06
FLOOR_SCORE = -1e30


def sent_together(arrays, axis, dim, along):
    widths = [a.shape[along] for a in arrays]
    both = jnp.concatenate(arrays, axis=along)
    result = lax.all_gather(both, axis, axis=dim, tiled=True)
    return tuple(jnp.split(result, [sum(widths[:k]) for k in range(1, len(widths))], axis=along))


def cut_along(shard, dim, size):
    before, after = (shard.shape[:dim], shard.shape[dim + 1 :])
    return jnp.moveaxis(shard.reshape(*before, size, -1, *after), dim, 0)


def summed_on_arrival(shard, axis, dim):
    size = lax.axis_size(axis)
    tiles = lax.all_to_all(cut_along(shard, dim, size), axis, 0, 0, tiled=True)
    return jnp.sum(tiles.astype(jnp.float32), axis=0)


def norm_rows(source, gain_vec):
    widened = source.astype(jnp.float32)
    return (
        widened
        * lax.rsqrt(jnp.mean(widened * widened, axis=-1, keepdims=True) + EPSILON)
        * gain_vec
    )


def rotate(source, positions):
    halfway = source.shape[-1] // 2
    frequency = 10000.0 ** (-jnp.arange(halfway, dtype=jnp.float32) / halfway)
    angles = positions.astype(jnp.float32)[:, None] * frequency[None, :]
    angles = angles.reshape((source.shape[0],) + (1,) * (source.ndim - 2) + (halfway,))
    cosine = jnp.cos(angles)
    sine_part = jnp.sin(angles)
    leading = source[..., :halfway]
    trailing = source[..., halfway:]
    return jnp.concatenate(
        [leading * cosine - trailing * sine_part, leading * sine_part + trailing * cosine], axis=-1
    )


def on_device(
    residual,
    query_latent,
    kv_latent,
    rotary_key,
    doc_ids,
    query_gain,
    kv_gain,
    w_query_nope,
    w_query_rot,
    w_key_nope,
    w_value,
    w_out,
    ffn_gain,
    w_gate,
    w_up,
    w_down,
    routes,
    group_weight,
    member_logits,
):
    queries_here = query_latent.shape[0]
    heads_here = w_key_nope.shape[1] // NOPE
    offset = lax.axis_index("sp") * queries_here
    query_pos = offset + jnp.arange(queries_here, dtype=jnp.int32)
    query_normed = norm_rows(query_latent, query_gain).astype(jnp.bfloat16)
    key_normed = norm_rows(kv_latent, kv_gain).astype(jnp.bfloat16)
    query_nope = jnp.dot(query_normed, w_query_nope, preferred_element_type=jnp.float32).astype(
        jnp.bfloat16
    )
    query_nope = query_nope.reshape(queries_here, heads_here, NOPE)
    query_rot = jnp.dot(query_normed, w_query_rot, preferred_element_type=jnp.float32)
    query_rot = rotate(query_rot.reshape(queries_here, heads_here, ROPE), query_pos).astype(
        jnp.bfloat16
    )
    key_rot = rotate(rotary_key.astype(jnp.float32), query_pos).astype(jnp.bfloat16)
    factor = (NOPE + ROPE) ** (-0.5)
    pieces = (
        *sent_together((key_normed, key_rot), "sp", 0, 1),
        lax.all_gather(doc_ids, "sp", axis=0, tiled=True),
    )
    key_nope = jnp.dot(pieces[0], w_key_nope, preferred_element_type=jnp.float32).astype(
        jnp.bfloat16
    )
    key_values = jnp.dot(pieces[0], w_value, preferred_element_type=jnp.float32).astype(
        jnp.bfloat16
    )
    key_count = key_nope.shape[0]
    scores = jnp.einsum(
        "qhd,khd->hqk",
        query_nope,
        key_nope.reshape(key_count, heads_here, NOPE),
        preferred_element_type=jnp.float32,
    )
    scores = (
        scores + jnp.einsum("qhr,kr->hqk", query_rot, pieces[1], preferred_element_type=jnp.float32)
    ) * factor
    key_pos = jnp.arange(key_count, dtype=jnp.int32)
    visible = (key_pos[None, :] <= query_pos[:, None]) & (pieces[2][None, :] == doc_ids[:, None])
    running = jnp.full((heads_here, queries_here), FLOOR_SCORE, jnp.float32)
    summed = jnp.zeros((queries_here, heads_here, VDIM), jnp.float32)
    highest = jnp.maximum(running, jnp.max(jnp.where(visible[None], scores, FLOOR_SCORE), axis=-1))
    weights = jnp.where(visible[None], jnp.exp(scores - highest[:, :, None]), 0.0)
    shrink = jnp.exp(running - highest)
    totals = jnp.sum(weights, axis=-1)
    summed = summed * shrink.T[:, :, None] + jnp.einsum(
        "hqk,khd->qhd",
        weights.astype(jnp.bfloat16),
        key_values.reshape(key_count, heads_here, VDIM),
        preferred_element_type=jnp.float32,
    )
    running, totals, summed = (highest, totals, summed)
    attended = (
        (summed / totals.T[:, :, None])
        .reshape(queries_here, heads_here * VDIM)
        .astype(jnp.bfloat16)
    )
    projected = summed_on_arrival(
        jnp.dot(attended, w_out, preferred_element_type=jnp.float32).astype(jnp.bfloat16), "tp", 0
    )
    after_mixer = (residual.astype(jnp.float32) + projected).astype(jnp.bfloat16)
    normed = norm_rows(after_mixer, ffn_gain).astype(jnp.bfloat16)
    experts = lax.axis_size("sp")
    groups_tp = lax.axis_size("tp")
    flat_routes = routes.reshape(-1)
    assigned = flat_routes.shape[0]
    capacity = assigned // experts
    onehot = (flat_routes[:, None] == jnp.arange(experts, dtype=jnp.int32)[None, :]).astype(
        jnp.int32
    )
    ranking = jnp.sum(onehot * (jnp.cumsum(onehot, axis=0) - 1), axis=1)
    slot_of = flat_routes * capacity + ranking
    source_of = (
        jnp.zeros((assigned,), jnp.int32).at[slot_of].set(jnp.arange(assigned, dtype=jnp.int32))
    )
    model_width = normed.shape[1]
    outgoing = normed[source_of // 2].reshape(experts, capacity, model_width)
    arrived = lax.all_to_all(outgoing, "sp", split_axis=0, concat_axis=0, tiled=True)
    arrived = lax.all_gather(arrived[:, None], "tp", axis=1, tiled=True)
    flat_rows = arrived.reshape(-1, model_width)
    gate_pre = jnp.dot(flat_rows, w_gate[0], preferred_element_type=jnp.float32)
    up_pre = jnp.dot(flat_rows, w_up[0], preferred_element_type=jnp.float32)
    hidden = (jax.nn.silu(gate_pre) * up_pre).astype(jnp.bfloat16)
    partial_value = jnp.dot(hidden, w_down[0], preferred_element_type=jnp.float32)
    partial_value = partial_value.reshape(experts, groups_tp, capacity, model_width)
    summed_back = summed_on_arrival(partial_value.astype(jnp.bfloat16), "tp", 1).astype(
        jnp.bfloat16
    )
    summed_back = summed_back.reshape(experts, capacity, model_width)
    returned = lax.all_to_all(summed_back, "sp", split_axis=0, concat_axis=0, tiled=True).reshape(
        experts * capacity, model_width
    )
    results = returned[slot_of].reshape(-1, 2, model_width).astype(jnp.float32)
    combine = group_weight[:, None] * jax.nn.softmax(member_logits, axis=-1)
    routed_sum = jnp.sum(combine[:, :, None] * results, axis=1)
    return (after_mixer.astype(jnp.float32) + routed_sum).astype(jnp.bfloat16)


def solution(mesh):
    return jax.shard_map(
        on_device,
        mesh=mesh,
        in_specs=(
            P(("grp", "sp", "tp"), None),
            P(("grp", "sp"), None),
            P(("grp", "sp"), None),
            P(("grp", "sp"), None),
            P(("grp", "sp")),
            P(),
            P(),
            P(None, "tp"),
            P(None, "tp"),
            P(None, "tp"),
            P(None, "tp"),
            P("tp", None),
            P(),
            P("sp", None, "tp"),
            P("sp", None, "tp"),
            P("sp", "tp", None),
            P(("grp", "sp", "tp"), None),
            P(("grp", "sp", "tp")),
            P(("grp", "sp", "tp"), None),
        ),
        out_specs=P(("grp", "sp", "tp"), None),
        check_vma=False,
    )
```

profile of v0, /device:TPU:33, one launch (start us, length us, event | category | flops | bytes accessed | tf_op | source)
XLA Modules:
  0.0 431.4 jit_solution(9626460216239463919)
XLA Ops:
  13.4 50.8 %all-gather.1 = s32[32,1,256]{2,1,0:T(1,128)S(1)} all-gather(s32[1,1,256]{2,1,0:T(1,128)} %bitcast.77), channel_id=1, replica_groups=mesh['grp'=2,'sp'=32,'tp'=4] {'sp'}, dimensions={0}, use_global_device_ids=true | all-gather | bytes 33792 | tf_op jit(solution)/shard_map/all_gather | solution.py:95
  65.7 3.5 fusion.8
  69.3 45.8 %all-gather.5.cloned.1.call-done = bf16[8192,448]{0,1:T(8,128)(2,1)} async-done(((bf16[256,448]{0,1:T(8,128)(2,1)}), bf16[8192,448]{0,1:T(8,128)(2,1)}) %all-gather.5.cloned.1.call-update) | async-done | bytes 7340048 | tf_op jit(solution)/shard_map/all_gather | solution.py:18
  115.1 6.2 %convolution_convert_fusion.1 = bf16[8192,384]{0,1:T(8,128)(2,1)S(1)} fusion(bf16[384,384]{1,0:T(8,128)(2,1)S(1)} %copy-done.8, bf16[8192,448]{0,1:T(8,128)(2,1)} %all-gather.5.cloned.1.call-done), kind=kOutput, calls=%fused_computation.14 | convolution fusion | flops 2419064832 | bytes 12877824 | tf_op jit(solution)/shard_map/dot_general | solution.py:97
  121.3 10.1 %fusion.56 = f32[3,256,8192]{2,1,0:T(8,128)} fusion(bf16[256,3,128]{0,2,1:T(8,128)(2,1)S(1)} %bitcast.73, bf16[8192,3,128]{0,2,1:T(8,128)(2,1)S(1)} %bitcast.70), kind=kOutput, calls=%fused_computation.96 | convolution fusion | flops 1610612736 | bytes 31653888 | tf_op jit(solution)/shard_map/qhd,khd->hqk/dot_general | solution.py:104
  131.4 17.0 %select_reduce_fusion = (f32[3,256]{1,0:T(4,128)S(1)}, f32[3,256,8192]{2,1,0:T(8,128)}) fusion(pred[256,8192]{1,0:T(8,128)(4,1)} %fusion.8, f32[3,256,8192]{2,1,0:T(8,128)} %fusion.56, bf16[256,3,32]{0,2,1:T(8,128)(2,1)S(1)} %get-tuple-element.8, bf16[256,3,32]{0,2,1:T(8,128)(2,1)S(1)} %get-tuple-element.7, bf16[8192,448]{0,1:T(8,128)(2,1)} %all-gather.5.cloned.1.call-done), kind=kOutput, calls=%fused_computation.6 | convolution fusion | flops 830668032 | bytes 53578752 | tf_op jit(solution)/shard_map/qhr,kr->hqk/dot_general | solution.py:111
  148.4 12.0 %fusion.1 = f32[3,256]{1,0:T(4,128)S(1)} fusion(f32[3,256,8192]{2,1,0:T(8,128)} %get-tuple-element.18, f32[3,256]{1,0:T(4,128)S(1)} %get-tuple-element.12, pred[256,8192]{1,0:T(8,128)(4,1)} %fusion.8), kind=kLoop, calls=%fused_computation.7 | loop fusion | flops 18873600 | bytes 27269120 | tf_op jit(solution)/shard_map/reduce_sum | solution.py:120
  160.4 9.0 %convolution_convert_fusion = bf16[8192,384]{0,1:T(8,128)(2,1)} fusion(bf16[384,384]{1,0:T(8,128)(2,1)S(1)} %copy-done.9, bf16[8192,448]{0,1:T(8,128)(2,1)} %all-gather.5.cloned.1.call-done), kind=kOutput, calls=%fused_computation.13 | convolution fusion | flops 2419064832 | bytes 12877824 | tf_op jit(solution)/shard_map/dot_general | solution.py:100
  169.4 13.3 %fusion.28 = bf16[256,3,128]{0,2,1:T(8,128)(2,1)S(1)} fusion(bf16[8192,3,128]{0,2,1:T(8,128)(2,1)} %bitcast.79, f32[3,256,8192]{2,1,0:T(8,128)} %get-tuple-element.18, f32[3,256]{1,0:T(4,128)S(1)} %get-tuple-element.12, pred[256,8192]{1,0:T(8,128)(4,1)} %fusion.8, f32[256,3]{0,1:T(4,128)S(1)} %bitcast.78, f32[256,3]{0,1:T(4,128)S(1)} %get-tuple-element.11), kind=kOutput, calls=%fused_computation.38 | convolution fusion | flops 1629782016 | bytes 33760256 | tf_op jit(solution)/shard_map/hqk,khd->qhd/dot_general | solution.py:121
  182.8 2.2 convolution_convert_fusion.3
  184.9 4.4 %all-to-all-start = ((bf16[4,64,3072]{2,1,0:T(8,128)(2,1)}), bf16[4,64,3072]{2,1,0:T(8,128)(2,1)}, u32[]{:S(2)}, u32[]{:S(2)}) async-start(bf16[4,64,3072]{2,1,0:T(8,128)(2,1)} %bitcast.69), calls=%async_computation | async-start | bytes 3145728 | tf_op jit(solution)/shard_map/all_to_all | solution.py:29
  191.4 18.5 %all-to-all-done = bf16[4,64,3072]{2,1,0:T(8,128)(2,1)} async-done(((bf16[4,64,3072]{2,1,0:T(8,128)(2,1)}), bf16[4,64,3072]{2,1,0:T(8,128)(2,1)}, u32[]{:S(2)}, u32[]{:S(2)}) %all-to-all-start) | async-done | bytes 1572896 | tf_op jit(solution)/shard_map/all_to_all | solution.py:29
  209.9 1.7 convert_reduce_fusion
  212.1 1.9 gather_fusion
  215.7 52.9 %all_to_all.20 = bf16[32,4,3072]{2,1,0:T(4,128)(2,1)S(1)} all-to-all(bf16[32,4,3072]{2,1,0:T(4,128)(2,1)S(1)} %reshape.218), channel_id=1, replica_groups=mesh['grp'=2,'sp'=32,'tp'=4] {'sp'}, dimensions={0} | all-to-all | bytes 1572864 | tf_op jit(solution)/shard_map/all_to_all | solution.py:153
  269.7 35.1 %all-gather.7.cloned.1.call-done = bf16[32,16,3072]{2,0,1:T(8,128)(2,1)} async-done(((bf16[32,4,3072]{2,0,1:T(8,128)(2,1)}), bf16[32,16,3072]{2,0,1:T(8,128)(2,1)}) %all-gather.7.cloned.1.call-update) | async-done | bytes 3145744 | tf_op jit(solution)/shard_map/all_gather | solution.py:154
  304.8 3.8 copy.76
  311.2 2.3 fusion.11
  313.5 39.3 %all_to_all.21 = bf16[4,32,1,4,3072]{4,1,3,2,0:T(8,128)(2,1)S(1)} all-to-all(bf16[4,32,1,4,3072]{4,1,3,2,0:T(8,128)(2,1)S(1)} %fusion.11), channel_id=1, replica_groups=mesh['grp'=2,'sp'=32,'tp'=4] {'tp'}, dimensions={0} | all-to-all | bytes 6291456 | tf_op jit(solution)/shard_map/all_to_all | solution.py:29
  354.8 14.4 %all-to-all-start.3 = ((bf16[32,4,3072]{2,1,0:T(4,128)(2,1)}), bf16[32,4,3072]{2,1,0:T(4,128)(2,1)}, u32[]{:S(2)}, u32[]{:S(2)}) async-start(bf16[32,4,3072]{2,1,0:T(4,128)(2,1)} %copy.81), calls=%async_computation.3 | async-start | bytes 1572864 | tf_op jit(solution)/shard_map/all_to_all | solution.py:165
  370.0 43.7 %all-to-all-done.3 = bf16[32,4,3072]{2,1,0:T(4,128)(2,1)} async-done(((bf16[32,4,3072]{2,1,0:T(4,128)(2,1)}), bf16[32,4,3072]{2,1,0:T(4,128)(2,1)}, u32[]{:S(2)}, u32[]{:S(2)}) %all-to-all-start.3) | async-done | bytes 786464 | tf_op jit(solution)/shard_map/all_to_all | solution.py:165
  415.3 1.9 gather_fusion.1
  417.2 3.0 reshape.222
  420.2 3.6 multiply_reduce_fusion
  (72 shorter events, 21.4 us)
Async XLA Ops:
  6.5 176.2 %copy-start = (bf16[384,3072]{1,0:T(8,128)(2,1)S(1)}, bf16[384,3072]{1,0:T(8,128)(2,1)}, u32[]{:S(2)}) copy-start(bf16[384,3072]{1,0:T(8,128)(2,1)} %param.30) | copy-start | bytes 7077892
  6.6 108.5 %copy-start.8 = (bf16[384,384]{1,0:T(8,128)(2,1)S(1)}, bf16[384,384]{1,0:T(8,128)(2,1)}, u32[]{:S(2)}) copy-start(bf16[384,384]{1,0:T(8,128)(2,1)} %param.28) | copy-start | bytes 884740
  6.6 108.5 %all-gather.5.cloned.1.call-start = ((), (), s32[]{:S(2)}) async-start(), calls=%async_computation.4 | async-start | bytes 7569408 | tf_op jit(solution)/shard_map/all_gather | solution.py:18
  148.4 12.0 %copy-start.9 = (bf16[384,384]{1,0:T(8,128)(2,1)S(1)}, bf16[384,384]{1,0:T(8,128)(2,1)}, u32[]{:S(2)}) copy-start(bf16[384,384]{1,0:T(8,128)(2,1)} %param.29) | copy-start | bytes 884740
  182.7 6.7 %copy-start.4 = (s32[64,2]{0,1:T(2,128)S(1)}, s32[64,2]{0,1:T(2,128)}, u32[]{:S(2)}) copy-start(s32[64,2]{0,1:T(2,128)} %param.35) | copy-start | bytes 1540
  182.7 28.9 %copy-start.1 = (bf16[64,3072]{1,0:T(8,128)(2,1)S(1)}, bf16[64,3072]{1,0:T(8,128)(2,1)}, u32[]{:S(2)}) copy-start(bf16[64,3072]{1,0:T(8,128)(2,1)} %param.19) | copy-start | bytes 1179652
  182.8 29.2 %copy-start.2 = (f32[3072]{0:T(1024)S(1)}, f32[3072]{0:T(1024)}, u32[]{:S(2)}) copy-start(f32[3072]{0:T(1024)} %param.31) | copy-start | bytes 36868
  184.9 25.0 %all-to-all-start = ((bf16[4,64,3072]{2,1,0:T(8,128)(2,1)}), bf16[4,64,3072]{2,1,0:T(8,128)(2,1)}, u32[]{:S(2)}, u32[]{:S(2)}) async-start(bf16[4,64,3072]{2,1,0:T(8,128)(2,1)} %bitcast.69), calls=%async_computation | async-start | bytes 3145728 | tf_op jit(solution)/shard_map/all_to_all | solution.py:29
  189.4 115.4 %all-gather.7.cloned.1.call-start = ((), (), s32[]{:S(2)}) async-start(), calls=%async_computation.5 | async-start | bytes 3932160 | tf_op jit(solution)/shard_map/all_gather | solution.py:154
  304.8 3.8 copy-start.6
  304.8 5.0 %copy-start.7 = (bf16[1,3072,192]{1,2,0:T(8,128)(2,1)S(1)}, bf16[1,3072,192]{1,2,0:T(8,128)(2,1)}, u32[]{:S(2)}) copy-start(bf16[1,3072,192]{1,2,0:T(8,128)(2,1)} %param.33) | copy-start | bytes 3538948
  313.5 55.8 %copy-start.3 = (f32[64,2]{0,1:T(2,128)S(1)}, f32[64,2]{0,1:T(2,128)}, u32[]{:S(2)}) copy-start(f32[64,2]{0,1:T(2,128)} %param.37) | copy-start | bytes 1540
  313.5 55.8 %copy-start.5 = (f32[64]{0:T(128)S(1)}, f32[64]{0:T(128)}, u32[]{:S(2)}) copy-start(f32[64]{0:T(128)} %param.36) | copy-start | bytes 772
  354.8 58.9 %all-to-all-start.3 = ((bf16[32,4,3072]{2,1,0:T(4,128)(2,1)}), bf16[32,4,3072]{2,1,0:T(4,128)(2,1)}, u32[]{:S(2)}, u32[]{:S(2)}) async-start(bf16[32,4,3072]{2,1,0:T(4,128)(2,1)} %copy.81), calls=%async_computation.3 | async-start | bytes 1572864 | tf_op jit(solution)/shard_map/all_to_all | solution.py:165
Sparse Core Ops, SparseCore 0:
  10.6 104.4 all-gather.4
  269.8 34.9 all-gather.6
where the time goes:
time: 432 us; the launch traced here: 431 us
  waiting for transfers between devices  143 us (33%)
  blocking collectives  143 us (33%)
  matrix products  65.5 us (15%)
  other arithmetic  27.1 us (6%)
  local copies, waits for them, and re-layouts  20.1 us (5%)
  starting transfers between devices  18.9 us (4%)
  between operations  13.8 us (3%)
    all_to_all x1, blocking collectives, on_device(): lax.all_to_all(outgoing, 'sp', split_axis=0, concat_axis=0, tiled=True)  52.9 us
    all_gather x1, blocking collectives, on_device(): lax.all_gather(doc_ids, 'sp', axis=0, tiled=True)  50.8 us
    all_gather x1, waiting for transfers between devices, sent_together(): result = lax.all_gather(both, axis, axis=dim, tiled=True)  45.8 us
    all_to_all x1, waiting for transfers between devices, on_device(): lax.all_to_all(summed_back, 'sp', split_axis=0, concat_axis=0, tiled=True)  43.7 us
    all_to_all x1, blocking collectives, summed_on_arrival(): tiles = lax.all_to_all(cut_along(shard, dim, size), axis, 0, 0, tiled=True)  39.3 us
    all_gather x1, waiting for transfers between devices, on_device(): arrived = lax.all_gather(arrived[:, None], 'tp', axis=1, tiled=True)  35.1 us
    all_to_all x1, waiting for transfers between devices, summed_on_arrival(): tiles = lax.all_to_all(cut_along(shard, dim, size), axis, 0, 0, tiled=True)  18.5 us
    dot_general x1, matrix products, on_device(): jnp.einsum('qhr,kr->hqk', query_rot, pieces[1], preferred_element_type=jn...  17 us
  transfers between devices with their start and end apart: 4, of which 4 were waited for; matrix products, arithmetic and copies ran while one was open for 2% of the time, Pallas kernels for 0%

commit v1 on v0

v1 whole, which is shorter than its diff:
```python
import functools

import jax
import jax.numpy as jnp
from jax import lax
from jax.experimental import pallas as pl
from jax.experimental.pallas import tpu as pltpu
from jax.sharding import PartitionSpec as P

NOPE = 128
ROPE = 64
VDIM = 128
DOC_MOST = 4352
N_DOCS = 4

EPSILON = 1e-06
FLOOR_SCORE = -1e30
MESH = pl.DeviceIdType.MESH
F32 = jnp.float32
BF16 = jnp.bfloat16


def norm_rows(source, gain_vec):
    widened = source.astype(F32)
    return (
        widened
        * lax.rsqrt(jnp.mean(widened * widened, axis=-1, keepdims=True) + EPSILON)
        * gain_vec
    )


def rotate(source, positions):
    halfway = source.shape[-1] // 2
    frequency = 10000.0 ** (-jnp.arange(halfway, dtype=F32) / halfway)
    angles = positions.astype(F32)[:, None] * frequency[None, :]
    angles = angles.reshape((source.shape[0],) + (1,) * (source.ndim - 2) + (halfway,))
    cosine = jnp.cos(angles)
    sine_part = jnp.sin(angles)
    leading = source[..., :halfway]
    trailing = source[..., halfway:]
    return jnp.concatenate(
        [leading * cosine - trailing * sine_part, leading * sine_part + trailing * cosine], axis=-1
    )


def dot(a, b):
    return jnp.dot(a, b, preferred_element_type=F32)


def attention_kernel(factor, index_ref, q_ref, kv_ref, wk_ref, wv_ref, out_ref, m_ref, l_ref, acc_ref):
    back = pl.program_id(0)
    latent_width = wk_ref.shape[0]
    heads, rows, _ = q_ref.shape

    def block(diagonal):
        latent = kv_ref[:, :latent_width]
        extra = kv_ref[:, latent_width:]
        key_nope = dot(latent, wk_ref[...]).astype(BF16)
        values = dot(latent, wv_ref[...]).astype(BF16)
        for h in range(heads):
            keys = jnp.concatenate([key_nope[:, h * NOPE : (h + 1) * NOPE], extra], axis=1)
            scores = lax.dot_general(
                q_ref[h], keys, (((1,), (1,)), ((), ())), preferred_element_type=F32
            )
            if diagonal:
                row = lax.broadcasted_iota(jnp.int32, scores.shape, 0)
                col = lax.broadcasted_iota(jnp.int32, scores.shape, 1)
                scores = jnp.where(col <= row, scores, FLOOR_SCORE)
            block_max = jnp.max(scores, axis=1, keepdims=True)
            value = values[:, h * VDIM : (h + 1) * VDIM]
            if diagonal:
                weights = jnp.exp((scores - block_max) * factor)
                m_ref[h] = block_max
                l_ref[h] = jnp.sum(weights, axis=1, keepdims=True)
                acc_ref[h] = dot(weights.astype(BF16), value)
            else:
                old = m_ref[h]
                highest = jnp.maximum(old, block_max)
                weights = jnp.exp((scores - highest) * factor)
                shrink = jnp.exp((old - highest) * factor)
                m_ref[h] = highest
                l_ref[h] = l_ref[h] * shrink + jnp.sum(weights, axis=1, keepdims=True)
                acc_ref[h] = acc_ref[h] * shrink + dot(weights.astype(BF16), value)

    @pl.when(back == 0)
    def _():
        block(True)

    @pl.when((back > 0) & (back <= index_ref[0]))
    def _():
        block(False)

    @pl.when(back == pl.num_programs(0) - 1)
    def _():
        for h in range(heads):
            out_ref[:, h * VDIM : (h + 1) * VDIM] = (acc_ref[h] / l_ref[h]).astype(out_ref.dtype)


def attention(index, queries, gathered, w_key, w_value):
    heads, rows, _ = queries.shape
    blocks = gathered.shape[0] // rows
    steps = min(blocks, 1 + (DOC_MOST + rows - 2) // rows)
    width = heads * VDIM
    return pl.pallas_call(
        functools.partial(attention_kernel, (NOPE + ROPE) ** (-0.5)),
        out_shape=jax.ShapeDtypeStruct((rows, width), BF16),
        grid_spec=pltpu.PrefetchScalarGridSpec(
            num_scalar_prefetch=1,
            grid=(steps,),
            in_specs=[
                pl.BlockSpec(queries.shape, lambda s, i: (0, 0, 0)),
                pl.BlockSpec(
                    (rows, gathered.shape[1]), lambda s, i: (lax.rem(i[0] - s + blocks, blocks), 0)
                ),
                pl.BlockSpec(w_key.shape, lambda s, i: (0, 0)),
                pl.BlockSpec(w_value.shape, lambda s, i: (0, 0)),
            ],
            out_specs=pl.BlockSpec((rows, width), lambda s, i: (0, 0)),
            scratch_shapes=[
                pltpu.VMEM((heads, rows, 1), F32),
                pltpu.VMEM((heads, rows, 1), F32),
                pltpu.VMEM((heads, rows, VDIM), F32),
            ],
        ),
        compiler_params=pltpu.CompilerParams(dimension_semantics=("arbitrary",)),
    )(index.reshape(1), queries, gathered, w_key, w_value)


COLS = 512
SPAN = 4


def offsets_of(chips):
    half, quarter = chips // 2, chips // 4
    offsets = [0, half, quarter, -quarter]
    for m in range(1, quarter):
        offsets += [m, -m, half - m, m - half]
    return offsets


def mixer_kernel(
    chips,
    att_ref, wout_ref, res_ref, gain_ref, meta_in, wg_hbm, wu_hbm, wd_hbm,
    out_ref,
    wg_ref, wu_ref, wd_ref, part, relay_l, relay_r, sum_r, sum_l, from_l, from_r, mixed,
    meta, tok, sendb, rec, back_t, back_rl, back_rr, back_sr, back_sl, back_fl, back_fr, zb, gb,
    yb, yrecv,
    wsem, pair_s, pair_r, ps, pr, zs, zr, xs, xr_, bs, br, gs, gr,
):
    sp = lax.axis_index("sp")
    x = lax.axis_index("tp")
    core = lax.rem(sp, 2)
    z = lax.div(sp, 2)
    partner = sp + 1 - 2 * core
    right, left, across = lax.rem(x + 1, 4), lax.rem(x + 3, 4), lax.rem(x + 2, 4)
    to_right, to_left, to_partner = {"tp": right}, {"tp": left}, {"sp": partner}
    offsets = offsets_of(chips)
    n_chunks = chips // SPAN
    rows, width = res_ref.shape
    half = width // 2

    def on_ring(offset):
        return {"sp": lax.rem(z + offset + chips, chips) * 2 + core}

    barrier = pltpu.get_barrier_semaphore()
    for target in [to_partner, to_left, to_right] + [on_ring(o) for o in offsets[1:]]:
        pl.semaphore_signal(barrier, inc=1, device_id=target, device_id_type=MESH)

    loads = [
        pltpu.make_async_copy(wg_hbm, wg_ref, wsem.at[0]),
        pltpu.make_async_copy(wu_hbm, wu_ref, wsem.at[1]),
        pltpu.make_async_copy(wd_hbm, wd_ref, wsem.at[2]),
    ]
    for load in loads:
        load.start()

    def remote(src, dst, ssem, rsem, target):
        return pltpu.make_async_remote_copy(
            src_ref=src, dst_ref=dst, send_sem=ssem, recv_sem=rsem, device_id=target,
            device_id_type=MESH,
        )

    def cols_of(t):
        return pl.ds(pl.multiple_of(t * COLS, COLS), COLS)

    def project(t, carry):
        value = dot(att_ref[...], wout_ref[:, cols_of(t)])
        part[:, :, cols_of(t)] = value.reshape(4, rows, COLS).astype(BF16)
        return carry

    sends = []

    def start(copy):
        copy.start()
        sends.append(copy)
        return copy

    lo, hi = pl.ds(0, half), pl.ds(half, half)
    tiles = width // COLS
    lax.fori_loop(0, tiles // 2, project, 0)
    pl.semaphore_wait(barrier, 3 + len(offsets) - 1)
    c_a = start(remote(part.at[across, :, lo], relay_l, ps.at[0], pr.at[0], to_right))
    c_d = start(remote(part.at[left, :, lo], from_r.at[:, lo], ps.at[1], pr.at[1], to_left))
    meta[core] = meta_in[...]
    m_x = start(remote(meta_in, meta.at[core], pair_s.at[0], pair_r.at[0], to_partner))
    lax.fori_loop(tiles // 2, tiles, project, 0)
    c_b = start(remote(part.at[across, :, hi], relay_r, ps.at[2], pr.at[2], to_left))
    c_c = start(remote(part.at[right, :, hi], from_l.at[:, hi], ps.at[3], pr.at[3], to_right))
    c_a.wait_recv()
    sum_r[...] = (part[right, :, :half].astype(F32) + relay_l[...].astype(F32)).astype(BF16)
    c_e = start(remote(sum_r, from_l.at[:, lo], ps.at[4], pr.at[4], to_right))
    c_b.wait_recv()
    sum_l[...] = (part[left, :, half:].astype(F32) + relay_r[...].astype(F32)).astype(BF16)
    c_f = start(remote(sum_l, from_r.at[:, hi], ps.at[5], pr.at[5], to_left))
    for copy in (c_d, c_c, c_e, c_f):
        copy.wait_recv()

    after = (
        res_ref[...].astype(F32)
        + (part[x].astype(F32) + from_l[...].astype(F32) + from_r[...].astype(F32))
    ).astype(BF16)
    mixed[...] = after
    tok[core] = norm_rows(after, gain_ref[...]).astype(BF16)
    t_x = start(remote(tok.at[core], tok.at[core], pair_s.at[1], pair_r.at[1], to_partner))
    m_x.wait_recv()
    keys = meta[...].reshape(2 * rows, meta.shape[2])
    slots = 8 * chips
    wanted = (lax.broadcasted_iota(jnp.int32, (2 * rows, slots), 1) + core * slots).astype(F32)
    first = keys[:, 0:1] == wanted
    second = keys[:, 1:2] == wanted
    choose = (first | second).astype(F32).astype(BF16)
    t_x.wait_recv()

    def select(t, carry):
        source = tok[:, :, cols_of(t)].reshape(2 * rows, COLS)
        picked = lax.dot_general(
            choose, source, (((0,), (0,)), ((), ())), preferred_element_type=F32
        )
        sendb[:, :, cols_of(t)] = picked.reshape(chips, 8, COLS).astype(BF16)
        return carry

    lax.fori_loop(0, tiles, select, 0)
    z_out = [None]
    for p in range(1, chips):
        z_out.append(
            start(
                remote(sendb.at[p], rec.at[x, p], zs.at[p], zr.at[p], on_ring(offsets[p]))
            )
        )
    rec[x, 0] = sendb[0]
    for load in loads:
        load.wait()

    fwd = [None] * n_chunks

    def spread(q):
        for p in range(q * SPAN, (q + 1) * SPAN):
            if p:
                z_out[p].wait_recv()
        whole = pl.ds(q * SPAN, SPAN)
        fwd[q] = [
            start(remote(rec.at[x, whole], rec.at[x, whole], xs.at[q, 0], xr_.at[q, 0], to_right)),
            start(remote(rec.at[x, whole], rec.at[x, whole], xs.at[q, 1], xr_.at[q, 1], to_left)),
        ]

    relays = [None] * n_chunks

    def relay(q):
        a = pl.ds(q * SPAN, SPAN // 2)
        b = pl.ds(q * SPAN + SPAN // 2, SPAN // 2)
        fwd[q][0].wait_recv()
        one = start(remote(rec.at[left, a], rec.at[left, a], xs.at[q, 2], xr_.at[q, 2], to_right))
        fwd[q][1].wait_recv()
        two = start(remote(rec.at[right, b], rec.at[right, b], xs.at[q, 3], xr_.at[q, 3], to_left))
        relays[q] = [one, two]

    backs = [None] * n_chunks
    lo2, hi2 = pl.ds(0, SPAN // 2), pl.ds(SPAN // 2, SPAN // 2)

    def experts(q):
        for copy in relays[q]:
            copy.wait_recv()
        many = 4 * SPAN * 8
        arrived = rec[:, q * SPAN : (q + 1) * SPAN].reshape(many, width)
        gate = dot(arrived, wg_ref[...])
        up = dot(arrived, wu_ref[...])
        hidden = (gate / (1.0 + jnp.exp(-gate)) * up).astype(BF16)

        def down(t, carry):
            value = dot(hidden, wd_ref[:, cols_of(t)])
            back_t[q, :, :, :, cols_of(t)] = value.reshape(4, SPAN, 8, COLS).astype(BF16)
            return carry

        lax.fori_loop(0, tiles, down, 0)
        own = back_t.at[q]
        backs[q] = [
            start(remote(own.at[across, lo2], back_rl.at[q], bs.at[q, 0], br.at[q, 0], to_right)),
            start(remote(own.at[across, hi2], back_rr.at[q], bs.at[q, 1], br.at[q, 1], to_left)),
            start(remote(own.at[right, hi2], back_fl.at[q, hi2], bs.at[q, 2], br.at[q, 2], to_right)),
            start(remote(own.at[left, lo2], back_fr.at[q, lo2], bs.at[q, 3], br.at[q, 3], to_left)),
        ]

    def add_relayed(q):
        backs[q][0].wait_recv()
        back_sr[q] = (
            back_t[q, right, : SPAN // 2].astype(F32) + back_rl[q].astype(F32)
        ).astype(BF16)
        backs[q].append(
            start(remote(back_sr.at[q], back_fl.at[q, lo2], bs.at[q, 4], br.at[q, 4], to_right))
        )
        backs[q][1].wait_recv()
        back_sl[q] = (
            back_t[q, left, SPAN // 2 :].astype(F32) + back_rr[q].astype(F32)
        ).astype(BF16)
        backs[q].append(
            start(remote(back_sl.at[q], back_fr.at[q, hi2], bs.at[q, 5], br.at[q, 5], to_left))
        )

    g_out = [None] * chips

    def give_back(q):
        for copy in backs[q][2:]:
            copy.wait_recv()
        zb[q] = (
            back_t[q, x].astype(F32) + back_fl[q].astype(F32) + back_fr[q].astype(F32)
        ).astype(BF16)
        for k in range(SPAN):
            p = q * SPAN + k
            if p:
                g_out[p] = start(
                    remote(zb.at[q, k], gb.at[p], gs.at[p], gr.at[p], on_ring(-offsets[p]))
                )
            else:
                gb[0] = zb[0, 0]

    stages = (spread, relay, experts, add_relayed, give_back)
    for tick in range(n_chunks + len(stages) - 1):
        for s in reversed(range(len(stages))):
            if 0 <= tick - s < n_chunks:
                stages[s](tick - s)

    for p in range(1, chips):
        g_out[p].wait_recv()
    weigh = jnp.where(first, keys[:, 2:3], 0.0) + jnp.where(second, keys[:, 3:4], 0.0)
    weigh_hi = weigh.astype(BF16)
    weigh_lo = (weigh - weigh_hi.astype(F32)).astype(BF16)

    def combine(t, carry):
        returned = gb[:, :, cols_of(t)].reshape(slots, COLS)
        yb[:, :, cols_of(t)] = (dot(weigh_hi, returned) + dot(weigh_lo, returned)).reshape(
            2, rows, COLS
        )
        return carry

    lax.fori_loop(0, tiles, combine, 0)
    y_x = start(remote(yb.at[1 - core], yrecv, pair_s.at[2], pair_r.at[2], to_partner))
    y_x.wait_recv()
    out_ref[...] = (mixed[...].astype(F32) + (yb[core] + yrecv[...])).astype(out_ref.dtype)
    for copy in sends:
        copy.wait_send()


def mixer(attended, w_out, residual, gain, meta, w_gate, w_up, w_down, chips):
    rows, width = residual.shape
    n_chunks = chips // SPAN
    vmem = pl.BlockSpec(memory_space=pltpu.VMEM)
    hbm = pl.BlockSpec(memory_space=pl.ANY)
    half = width // 2
    dma = pltpu.SemaphoreType.DMA
    chunk = (n_chunks, SPAN, 8, width)
    half_chunk = (n_chunks, SPAN // 2, 8, width)
    return pl.pallas_call(
        functools.partial(mixer_kernel, chips),
        out_shape=jax.ShapeDtypeStruct((rows, width), BF16),
        in_specs=[vmem] * 5 + [hbm] * 3,
        out_specs=vmem,
        scratch_shapes=[
            pltpu.VMEM(w_gate.shape, BF16),
            pltpu.VMEM(w_up.shape, BF16),
            pltpu.VMEM(w_down.shape, BF16),
            pltpu.VMEM((4, rows, width), BF16),
            pltpu.VMEM((rows, half), BF16),
            pltpu.VMEM((rows, half), BF16),
            pltpu.VMEM((rows, half), BF16),
            pltpu.VMEM((rows, half), BF16),
            pltpu.VMEM((rows, width), BF16),
            pltpu.VMEM((rows, width), BF16),
            pltpu.VMEM((rows, width), BF16),
            pltpu.VMEM((2, rows, meta.shape[1]), F32),
            pltpu.VMEM((2, rows, width), BF16),
            pltpu.VMEM((chips, 8, width), BF16),
            pltpu.VMEM((4, chips, 8, width), BF16),
            pltpu.VMEM((n_chunks, 4, SPAN, 8, width), BF16),
            pltpu.VMEM(half_chunk, BF16),
            pltpu.VMEM(half_chunk, BF16),
            pltpu.VMEM(half_chunk, BF16),
            pltpu.VMEM(half_chunk, BF16),
            pltpu.VMEM(chunk, BF16),
            pltpu.VMEM(chunk, BF16),
            pltpu.VMEM(chunk, BF16),
            pltpu.VMEM((chips, 8, width), BF16),
            pltpu.VMEM((2, rows, width), F32),
            pltpu.VMEM((rows, width), F32),
            dma((3,)),
            dma((3,)),
            dma((3,)),
            dma((6,)),
            dma((6,)),
            dma((chips,)),
            dma((chips,)),
            dma((n_chunks, 4)),
            dma((n_chunks, 4)),
            dma((n_chunks, 6)),
            dma((n_chunks, 6)),
            dma((chips,)),
            dma((chips,)),
        ],
        compiler_params=pltpu.CompilerParams(
            collective_id=0, has_side_effects=True, vmem_limit_bytes=56 * 1024 * 1024
        ),
    )(attended, w_out, residual, gain, meta, w_gate, w_up, w_down)


def routing_meta(routes, group_weight, member_logits, chips):
    sp = lax.axis_index("sp")
    core, z = sp % 2, sp // 2
    flat = routes.reshape(-1)
    count = flat.shape[0]
    earlier = jnp.arange(count)[None, :] < jnp.arange(count)[:, None]
    same = flat[:, None] == flat[None, :]
    ranking = jnp.sum((same & earlier).astype(jnp.int32), axis=1).reshape(routes.shape)
    distance = (routes // 2 - z + chips) % chips
    position = jnp.zeros_like(routes)
    for p, offset in enumerate(offsets_of(chips)):
        position = jnp.where(distance == offset % chips, p, position)
    key = (routes % 2) * (8 * chips) + position * 8 + core * 4 + ranking
    weights = group_weight[:, None] * jax.nn.softmax(member_logits, axis=-1)
    filler = jnp.zeros((routes.shape[0], 124), F32)
    return jnp.concatenate([key.astype(F32), weights, filler], axis=1)


def on_device(
    residual,
    query_latent,
    kv_latent,
    rotary_key,
    doc_ids,
    query_gain,
    kv_gain,
    w_query_nope,
    w_query_rot,
    w_key_nope,
    w_value,
    w_out,
    ffn_gain,
    w_gate,
    w_up,
    w_down,
    routes,
    group_weight,
    member_logits,
):
    queries_here = query_latent.shape[0]
    heads_here = w_key_nope.shape[1] // NOPE
    index = lax.axis_index("sp")
    chips = lax.axis_size("sp") // 2
    query_pos = index * queries_here + jnp.arange(queries_here, dtype=jnp.int32)
    is_doc = doc_ids[:, None] == jnp.arange(ROPE, dtype=jnp.int32)[None, :]
    key_normed = norm_rows(kv_latent, kv_gain).astype(BF16)
    key_rot = rotate(rotary_key.astype(F32), query_pos).astype(BF16)
    own = jnp.concatenate([key_normed, key_rot, is_doc.astype(BF16)], axis=1)
    gathered = lax.all_gather(own, "sp", axis=0, tiled=True)

    query_normed = norm_rows(query_latent, query_gain).astype(BF16)
    query_nope = dot(query_normed, w_query_nope).astype(BF16)
    query_nope = query_nope.reshape(queries_here, heads_here, NOPE)
    query_rot = dot(query_normed, w_query_rot).reshape(queries_here, heads_here, ROPE)
    query_rot = rotate(query_rot, query_pos).astype(BF16)
    other_doc = jnp.where(is_doc, 0.0, FLOOR_SCORE).astype(BF16)
    other_doc = jnp.broadcast_to(other_doc[:, None, :], query_rot.shape)
    queries = jnp.concatenate([query_nope, query_rot, other_doc], axis=2).transpose(1, 0, 2)

    attended = attention(index, queries, gathered, w_key_nope, w_value)
    meta = routing_meta(routes, group_weight, member_logits, chips)
    return mixer(
        attended, w_out, residual, ffn_gain[None, :], meta, w_gate[0], w_up[0], w_down[0], chips
    )


def solution(mesh):
    return jax.shard_map(
        on_device,
        mesh=mesh,
        in_specs=(
            P(("grp", "sp", "tp"), None),
            P(("grp", "sp"), None),
            P(("grp", "sp"), None),
            P(("grp", "sp"), None),
            P(("grp", "sp")),
            P(),
            P(),
            P(None, "tp"),
            P(None, "tp"),
            P(None, "tp"),
            P(None, "tp"),
            P("tp", None),
            P(),
            P("sp", None, "tp"),
            P("sp", None, "tp"),
            P("sp", "tp", None),
            P(("grp", "sp", "tp"), None),
            P(("grp", "sp", "tp")),
            P(("grp", "sp", "tp"), None),
        ),
        out_specs=P(("grp", "sp", "tp"), None),
        check_vma=False,
    )
```

time: 432 us -> 275 us (0.64)
  Pallas kernels: 0 us -> 162 us
  blocking collectives: 143 us -> 0 us
  matrix products: 65.5 us -> 0.79 us
  waiting for transfers between devices: 143 us -> 83.4 us
  other arithmetic: 27.1 us -> 6.63 us
  starting transfers between devices: 18.9 us -> 0.06 us
  local copies, waits for them, and re-layouts: 20.1 us -> 8.35 us
    pallas_call x0 -> x2, Pallas kernels: none -> 162 us  [the longest x1 149 us: mixer(): pl.pallas_call(functools.partial(mixer_kernel, chips), out_shape=jax.Shap...]
    all_to_all x2 -> x0, blocking collectives: 92.1 us -> none  [the longest x1 52.9 us: on_device(): lax.all_to_all(outgoing, 'sp', split_axis=0, concat_axis=0, tiled=True)]
    dot_general x11 -> x2, matrix products: 65.5 us -> 0.79 us  [dot(): return jnp.dot(a, b, preferred_element_type=F32)]
    all_to_all x2 -> x0, waiting for transfers between devices: 62.2 us -> none  [the longest x1 43.7 us: on_device(): lax.all_to_all(summed_back, 'sp', split_axis=0, concat_axis=0, tiled=True)]
    all_gather x1 -> x0, blocking collectives: 50.8 us -> none  [on_device(): lax.all_gather(doc_ids, 'sp', axis=0, tiled=True)]
    all_to_all x2 -> x0, starting transfers between devices: 18.8 us -> none  [the longest x1 14.4 us: on_device(): lax.all_to_all(summed_back, 'sp', split_axis=0, concat_axis=0, tiled=True)]
    reduce_sum x6 -> x2, other arithmetic: 18 us -> 0.2 us  [the longest x1 0.18 us: routing_meta(): jnp.sum((same & earlier).astype(jnp.int32), axis=1).reshape(routes.shape)]
    unnamed x22 -> x25, local copies, waits for them, and re-layouts: 1.21 us -> 7.44 us
  transfers between devices with their start and end apart: 4 -> 1, of which waited for: 4 -> 1; matrix products, arithmetic and copies ran while one was open for 2% -> 3% of each run, Pallas kernels for 0% -> 0%
where the time goes in v1:
time: 275 us
  Pallas kernels  162 us (59%)
  waiting for transfers between devices  83.4 us (30%)
  between operations  13.7 us (5%)
  local copies, waits for them, and re-layouts  8.35 us (3%)
  other arithmetic  6.63 us (2%)
    pallas_call x1, Pallas kernels, mixer(): pl.pallas_call(functools.partial(mixer_kernel, chips), out_shape=jax.Shap...  149 us
    all_gather x1, waiting for transfers between devices, on_device(): gathered = lax.all_gather(own, 'sp', axis=0, tiled=True)  83.3 us
    pallas_call x1, Pallas kernels, attention(): pl.pallas_call(functools.partial(attention_kernel, (NOPE + ROPE) ** (-0.5...  13.1 us
    unnamed x25, local copies, waits for them, and re-layouts  7.44 us
  transfers between devices with their start and end apart: 1, of which 1 were waited for; matrix products, arithmetic and copies ran while one was open for 3% of the time, Pallas kernels for 0%

profile of v1, /device:TPU:33, one launch (start us, length us, event | category | flops | bytes accessed | tf_op | source)
XLA Modules:
  0.0 274.7 jit_solution(10791222676620878931)
XLA Ops:
  6.6 1.0 copy.81
  7.6 0.8 fusion.6
  8.4 1.0 fusion.3
  9.5 1.0 fusion.5
  10.5 0.6 subtract_convert_fusion.1
  11.1 0.8 pad_maximum_fusion
  12.0 0.2 fusion
  12.2 0.4 fusion.7
  12.6 0.2 copy.96
  12.8 0.2 copy.95
  13.0 0.4 convolution_convert_fusion
  13.4 0.1 copy.76
  13.6 0.2 copy.80
  14.0 0.1 eq.133
  14.1 0.2 convert_reduce_fusion
  14.3 0.1 reshape.118
  14.7 1.7 copy.92
  16.4 2.5 copy.93
  19.2 0.9 maximum_bitcast_fusion.q_ref
  20.2 0.7 maximum_maximum_fusion.meta_in
  20.9 83.3 %all-gather.2.cloned.1.call-done.kv_ref = bf16[8192,512]{1,0:T(8,128)(2,1)} async-done(((bf16[256,512]{1,0:T(8,128)(2,1)}), bf16[8192,512]{1,0:T(8,128)(2,1)}) %all-gather.2.cloned.1.call-update) | async-done | bytes 8388624 | tf_op jit(solution)/shard_map/all_gather | solution.py:472
  104.3 13.1 %shard_map.181.att_ref = bf16[256,384]{1,0:T(8,128)(2,1)} custom-call(s32[1]{0:T(128)} %bitcast.index_ref, bf16[3,256,256]{2,1,0:T(8,128)(2,1)} %maximum_bitcast_fusion.q_ref, bf16[8192,512]{1,0:T(8,128)(2,1)} %all-gather.2.cloned.1.call-done.kv_ref, bf16[384,384]{1,0:T(8,128)(2,1)} %wk_ref.1, bf16[384,384]{1,0:T(8,128)(2,1)} %wv_ref.1), custom_call_target="tpu_custom_call" | custom-call | tf_op jit(solution)/shard_map/pallas_call | solution.py:104
  117.4 148.7 %shard_map.182 = bf16[64,3072]{1,0:T(8,128)(2,1)} custom-call(bf16[256,384]{1,0:T(8,128)(2,1)} %shard_map.181.att_ref, bf16[384,3072]{1,0:T(8,128)(2,1)} %wout_ref.1, bf16[64,3072]{1,0:T(8,128)(2,1)} %res_ref.1, f32[1,3072]{1,0:T(1,128)} %bitcast.16, f32[64,128]{1,0:T(8,128)} %maximum_maximum_fusion.meta_in, bf16[3072,192]{1,0:T(8,128)(2,1)} %bitcast.11, ...), custom_call_target="tpu_custom_call" | custom-call | tf_op jit(solution)/shard_map/pallas_call | solution.py:372
  266.1 1.8 copy.102
  (39 shorter events, 1.0 us)
Async XLA Ops:
  6.5 6.4 %copy-start = (bf16[768,384]{1,0:T(8,128)(2,1)S(1)}, bf16[768,384]{1,0:T(8,128)(2,1)}, u32[]{:S(2)}) copy-start(bf16[768,384]{1,0:T(8,128)(2,1)} %param.26) | copy-start | bytes 1769476
  6.6 5.5 %copy-start.2 = (bf16[256,768]{1,0:T(8,128)(2,1)S(1)}, bf16[256,768]{1,0:T(8,128)(2,1)}, u32[]{:S(2)}) copy-start(bf16[256,768]{1,0:T(8,128)(2,1)} %param.20) | copy-start | bytes 1179652
  6.6 5.6 %copy-start.7 = (bf16[768,192]{0,1:T(8,128)(2,1)S(1)}, bf16[768,192]{0,1:T(8,128)(2,1)}, u32[]{:S(2)}) copy-start(bf16[768,192]{0,1:T(8,128)(2,1)} %param.27) | copy-start | bytes 884740
  6.6 5.6 %copy-start.8 = (f32[768]{0:T(1024)S(1)}, f32[768]{0:T(1024)}, u32[]{:S(2)}) copy-start(f32[768]{0:T(1024)} %param.24) | copy-start | bytes 9220
  6.6 97.7 %all-gather.2.cloned.1.call-start = ((), (), s32[]{:S(2)}) async-start(), calls=%async_computation | async-start | bytes 8650752 | tf_op jit(solution)/shard_map/all_gather | solution.py:472
  12.6 1.1 copy-start.3
  12.6 1.2 copy-start.6
  12.6 1.3 copy-start.5
  12.8 1.9 copy-start.1
  16.4 2.5 copy-start.4
Sparse Core Ops, SparseCore 0:
  12.1 92.1 all-gather.1

commit v2 on v1

--- a/solution.py
+++ b/solution.py
@@ -1,4 +1,5 @@
 import functools
+import math
 
 import jax
 import jax.numpy as jnp
@@ -11,7 +12,6 @@
 ROPE = 64
 VDIM = 128
 DOC_MOST = 4352
-N_DOCS = 4
 
 EPSILON = 1e-06
 FLOOR_SCORE = -1e30
@@ -29,101 +29,302 @@
     )
 
 
-def rotate(source, positions):
-    halfway = source.shape[-1] // 2
-    frequency = 10000.0 ** (-jnp.arange(halfway, dtype=F32) / halfway)
-    angles = positions.astype(F32)[:, None] * frequency[None, :]
-    angles = angles.reshape((source.shape[0],) + (1,) * (source.ndim - 2) + (halfway,))
-    cosine = jnp.cos(angles)
-    sine_part = jnp.sin(angles)
-    leading = source[..., :halfway]
-    trailing = source[..., halfway:]
-    return jnp.concatenate(
-        [leading * cosine - trailing * sine_part, leading * sine_part + trailing * cosine], axis=-1
-    )
-
-
 def dot(a, b):
     return jnp.dot(a, b, preferred_element_type=F32)
 
 
-def attention_kernel(factor, index_ref, q_ref, kv_ref, wk_ref, wv_ref, out_ref, m_ref, l_ref, acc_ref):
-    back = pl.program_id(0)
+def dot_nt(a, b):
+    return lax.dot_general(a, b, (((1,), (1,)), ((), ())), preferred_element_type=F32)
+
+
+def attention_kernel(
+    factor, hops, seed,
+    ql_ref, kl_ref, rk_ref, doc_ref, qg_ref, kg_ref, wqn_ref, wqr_ref, wk_ref, wv_ref,
+    out_ref,
+    kv, keys_ref, values_ref, q_ref, m_ref, l_ref, acc_ref, zs, zr, xs, xr_, ds, dr,
+):
+    sp = lax.axis_index("sp")
+    n_sp = lax.axis_size("sp")
+    x = lax.axis_index("tp")
+    core = lax.rem(sp, 2)
+    z = lax.div(sp, 2)
+    right, left, across = lax.rem(x + 1, 4), lax.rem(x + 3, 4), lax.rem(x + 2, 4)
+    to_right, to_left, to_partner = {"tp": right}, {"tp": left}, {"sp": sp + 1 - 2 * core}
+
+    def chip_at(offset):
+        return {"sp": lax.rem(sp + 2 * offset + n_sp, n_sp)}
+
+    rows = ql_ref.shape[0]
+    heads = q_ref.shape[0]
     latent_width = wk_ref.shape[0]
-    heads, rows, _ = q_ref.shape
-
-    def block(diagonal):
-        latent = kv_ref[:, :latent_width]
-        extra = kv_ref[:, latent_width:]
-        key_nope = dot(latent, wk_ref[...]).astype(BF16)
-        values = dot(latent, wv_ref[...]).astype(BF16)
-        for h in range(heads):
-            keys = jnp.concatenate([key_nope[:, h * NOPE : (h + 1) * NOPE], extra], axis=1)
-            scores = lax.dot_general(
-                q_ref[h], keys, (((1,), (1,)), ((), ())), preferred_element_type=F32
+    quarter = rows // 4
+
+    barrier = pltpu.get_barrier_semaphore()
+    greeted = [to_partner, to_left, to_right] + [chip_at(o) for o in (1, -1, seed, -seed)]
+    for target in greeted:
+        pl.semaphore_signal(barrier, inc=1, device_id=target, device_id_type=MESH)
+
+    def remote(src, dst, ssem, rsem, target):
+        return pltpu.make_async_remote_copy(
+            src_ref=src, dst_ref=dst, send_sem=ssem, recv_sem=rsem, device_id=target,
+            device_id_type=MESH,
+        )
+
+    def onward(h):
+        return remote(
+            kv.at[h, core, x], kv.at[h + 1, core, x], zs.at[h + 1], zr.at[h + 1], chip_at(1)
+        )
+
+    def jump():
+        return remote(
+            kv.at[0, core, x], kv.at[seed, core, x], zs.at[seed], zr.at[seed], chip_at(seed)
+        )
+
+    def beside(h, k):
+        owner = (x, x, left, right)[k]
+        target = (to_right, to_left, to_right, to_left)[k]
+        part = kv.at[h, core, owner]
+        if k >= 2:
+            part = part.at[pl.ds((k - 2) * (quarter // 2), quarter // 2)]
+        return remote(part, part, xs.at[h, k], xr_.at[h, k], target)
+
+    def shared(h):
+        return [
+            remote(
+                r.at[h, core], r.at[h, core], ds.at[h, k], dr.at[h, k], to_partner
             )
-            if diagonal:
-                row = lax.broadcasted_iota(jnp.int32, scores.shape, 0)
-                col = lax.broadcasted_iota(jnp.int32, scores.shape, 1)
-                scores = jnp.where(col <= row, scores, FLOOR_SCORE)
-            block_max = jnp.max(scores, axis=1, keepdims=True)
-            value = values[:, h * VDIM : (h + 1) * VDIM]
-            if diagonal:
-                weights = jnp.exp((scores - block_max) * factor)
-                m_ref[h] = block_max
-                l_ref[h] = jnp.sum(weights, axis=1, keepdims=True)
-                acc_ref[h] = dot(weights.astype(BF16), value)
-            else:
-                old = m_ref[h]
-                highest = jnp.maximum(old, block_max)
-                weights = jnp.exp((scores - highest) * factor)
+            for k, r in enumerate((keys_ref, values_ref))
+        ]
+
+    step = -math.log(10000.0) / (ROPE // 2)
+    frequency = jnp.exp(
+        lax.broadcasted_iota(jnp.int32, (ROPE // 2, rows), 0).astype(F32) * step
+    )
+    position = (sp * rows + lax.broadcasted_iota(jnp.int32, (ROPE // 2, rows), 1)).astype(F32)
+    angles = position * frequency
+    cosine, sine = jnp.cos(angles), jnp.sin(angles)
+
+    def turned(source):
+        a, b = source[: ROPE // 2], source[ROPE // 2 :]
+        return jnp.concatenate([a * cosine - b * sine, a * sine + b * cosine], axis=0)
+
+    docs = jnp.broadcast_to(doc_ref[...], (ROPE, rows))
+    same_doc = docs == lax.broadcasted_iota(jnp.int32, (ROPE, rows), 0)
+    key_tail = jnp.concatenate(
+        [turned(rk_ref[...].astype(F32)), same_doc.astype(F32)], axis=0
+    ).T.astype(BF16)
+    latent = norm_rows(kl_ref[...], kg_ref[...][None, :]).astype(BF16)
+    own = jnp.concatenate([latent, key_tail], axis=1)
+    kv[0, core] = own.reshape(4, quarter, own.shape[1])
+    pl.semaphore_wait(barrier, len(greeted))
+    onward(0).start()
+    jump().start()
+
+    def project(h):
+        block = kv[h, core].reshape(rows, kv.shape[-1])
+        latent = block[:, :latent_width]
+        keys_ref[h, core, :, :latent_width] = dot(latent, wk_ref[...]).astype(BF16)
+        keys_ref[h, core, :, latent_width:] = block[:, latent_width:]
+        values_ref[h, core] = lax.dot_general(
+            wv_ref[...], latent, (((0,), (1,)), ((), ())), preferred_element_type=F32
+        ).astype(BF16)
+        for copy in shared(h):
+            copy.start()
+
+    project(0)
+
+    query_normed = norm_rows(ql_ref[...], qg_ref[...][None, :]).astype(BF16)
+    nope = lax.dot_general(
+        wqn_ref[...], query_normed, (((0,), (1,)), ((), ())), preferred_element_type=F32
+    )
+    rot = dot_nt(wqr_ref[...], query_normed)
+    reject = jnp.where(same_doc, 0.0, FLOOR_SCORE)
+    for h in range(heads):
+        q_ref[h] = jnp.concatenate(
+            [nope[h * NOPE : (h + 1) * NOPE], turned(rot[h * ROPE : (h + 1) * ROPE]), reject],
+            axis=0,
+        ).astype(BF16)
+
+    def attend(h, blocks, diagonal):
+        scores, values = [], []
+        for b in blocks:
+            keys = keys_ref[h, b]
+            tail = keys[:, latent_width:]
+            values.append(values_ref[h, b])
+            scores.append([
+                dot(
+                    jnp.concatenate([keys[:, i * NOPE : (i + 1) * NOPE], tail], axis=1), q_ref[i]
+                )
+                for i in range(heads)
+            ])
+        if diagonal:
+            shape = (rows, rows)
+            col = core * rows + lax.broadcasted_iota(jnp.int32, shape, 1)
+            row = lax.broadcasted_iota(jnp.int32, shape, 0)
+            scores = [
+                [jnp.where(row + k * rows <= col, s, FLOOR_SCORE) for s in block]
+                for k, block in enumerate(scores)
+            ]
+        for i in range(heads):
+            mine = [block[i] for block in scores]
+            highest = functools.reduce(
+                jnp.maximum, [jnp.max(s, axis=0, keepdims=True) for s in mine]
+            )
+            if not diagonal:
+                old = m_ref[i]
+                highest = jnp.maximum(old, highest)
+            weights = [jnp.exp((s - highest) * factor) for s in mine]
+            total = sum(jnp.sum(w, axis=0, keepdims=True) for w in weights)
+            attended = sum(
+                dot(v[i * VDIM : (i + 1) * VDIM], w.astype(BF16)) for v, w in zip(values, weights)
+            )
+            if not diagonal:
                 shrink = jnp.exp((old - highest) * factor)
-                m_ref[h] = highest
-                l_ref[h] = l_ref[h] * shrink + jnp.sum(weights, axis=1, keepdims=True)
-                acc_ref[h] = acc_ref[h] * shrink + dot(weights.astype(BF16), value)
-
-    @pl.when(back == 0)
+                total = l_ref[i] * shrink + total
+                attended = acc_ref[i] * shrink + attended
+            m_ref[i] = highest
+            l_ref[i] = total
+            acc_ref[i] = attended
+
+    def hop_at(n):
+        return jnp.where(n == hops, n, jnp.where(n % 2 == 1, (n + 1) // 2, seed - 1 + n // 2))
+
+    def held(n):
+        return (n >= 1) & ((n < hops) | ((n == hops) & (core == 1)))
+
+    def goes_on(h):
+        return (h != seed - 1) & ((h < hops - 1) | ((h == hops - 1) & (core == 1)))
+
+    def arrive(n):
+        @pl.when(held(n))
+        def _():
+            h = hop_at(n)
+            onward(h - 1).wait_recv()
+
+            @pl.when(goes_on(h))
+            def _():
+                onward(h).start()
+
+            beside(h, 0).start()
+            beside(h, 1).start()
+
+    def pass_on(n):
+        @pl.when(held(n))
+        def _():
+            h = hop_at(n)
+            beside(h, 0).wait_recv()
+            beside(h, 2).start()
+            beside(h, 1).wait_recv()
+            beside(h, 3).start()
+
+    def share(n):
+        @pl.when(held(n))
+        def _():
+            h = hop_at(n)
+            beside(h, 2).wait_recv()
+            beside(h, 3).wait_recv()
+            project(h)
+
+    def use(n):
+        @pl.when((n >= 1) & (n < hops))
+        def _():
+            h = hop_at(n)
+            for copy in shared(h):
+                copy.wait_recv()
+
+            @pl.when(h <= z)
+            def _():
+                attend(h, (0, 1), False)
+
+    arrive(1)
+    for copy in shared(0):
+        copy.wait_recv()
+    attend(0, (0, 1), True)
+
+    def tick(t, carry):
+        arrive(t)
+        pass_on(t - 1)
+        share(t - 2)
+        use(t - 3)
+        return carry
+
+    lax.fori_loop(2, hops + 3, tick, 0)
+
+    @pl.when(core == 0)
     def _():
-        block(True)
-
-    @pl.when((back > 0) & (back <= index_ref[0]))
-    def _():
-        block(False)
-
-    @pl.when(back == pl.num_programs(0) - 1)
-    def _():
-        for h in range(heads):
-            out_ref[:, h * VDIM : (h + 1) * VDIM] = (acc_ref[h] / l_ref[h]).astype(out_ref.dtype)
-
-
-def attention(index, queries, gathered, w_key, w_value):
-    heads, rows, _ = queries.shape
-    blocks = gathered.shape[0] // rows
-    steps = min(blocks, 1 + (DOC_MOST + rows - 2) // rows)
+        for copy in shared(hops):
+            copy.wait_recv()
+
+        @pl.when(hops <= z)
+        def _():
+            attend(hops, (1,), False)
+
+    for i in range(heads):
+        out_ref[:, i * VDIM : (i + 1) * VDIM] = (acc_ref[i] / l_ref[i]).T.astype(out_ref.dtype)
+
+    onward(0).wait_send()
+    jump().wait_send()
+    for copy in shared(0):
+        copy.wait_send()
+
+    def drain(h, carry):
+        @pl.when(held(h))
+        def _():
+            @pl.when(goes_on(h))
+            def _():
+                onward(h).wait_send()
+
+            for k in range(4):
+                beside(h, k).wait_send()
+            for copy in shared(h):
+                copy.wait_send()
+
+        return carry
+
+    lax.fori_loop(1, hops + 1, drain, 0)
+
+
+def attention(
+    query_latent, kv_latent, rotary_key, doc_ids, query_gain, kv_gain, w_query_nope, w_query_rot,
+    w_key, w_value,
+):
+    rows = query_latent.shape[0]
+    heads = w_key.shape[1] // NOPE
     width = heads * VDIM
+    latent_width = kv_latent.shape[1]
+    blocks_back = (DOC_MOST + rows - 2) // rows
+    hops = (blocks_back + 1) // 2
+    assert blocks_back % 2 == 1 and hops % 2 == 1
+    seed = (hops + 1) // 2
+    vmem = pl.BlockSpec(memory_space=pltpu.VMEM)
+    dma = pltpu.SemaphoreType.DMA
     return pl.pallas_call(
-        functools.partial(attention_kernel, (NOPE + ROPE) ** (-0.5)),
+        functools.partial(attention_kernel, (NOPE + ROPE) ** (-0.5), hops, seed),
         out_shape=jax.ShapeDtypeStruct((rows, width), BF16),
-        grid_spec=pltpu.PrefetchScalarGridSpec(
-            num_scalar_prefetch=1,
-            grid=(steps,),
-            in_specs=[
-                pl.BlockSpec(queries.shape, lambda s, i: (0, 0, 0)),
-                pl.BlockSpec(
-                    (rows, gathered.shape[1]), lambda s, i: (lax.rem(i[0] - s + blocks, blocks), 0)
-                ),
-                pl.BlockSpec(w_key.shape, lambda s, i: (0, 0)),
-                pl.BlockSpec(w_value.shape, lambda s, i: (0, 0)),
-            ],
-            out_specs=pl.BlockSpec((rows, width), lambda s, i: (0, 0)),
-            scratch_shapes=[
-                pltpu.VMEM((heads, rows, 1), F32),
-                pltpu.VMEM((heads, rows, 1), F32),
-                pltpu.VMEM((heads, rows, VDIM), F32),
-            ],
+        in_specs=[vmem] * 10,
+        out_specs=vmem,
+        scratch_shapes=[
+            pltpu.VMEM((hops + 1, 2, 4, rows // 4, latent_width + 2 * ROPE), BF16),
+            pltpu.VMEM((hops + 1, 2, rows, width + 2 * ROPE), BF16),
+            pltpu.VMEM((hops + 1, 2, width, rows), BF16),
+            pltpu.VMEM((heads, 2 * NOPE, rows), BF16),
+            pltpu.VMEM((heads, 1, rows), F32),
+            pltpu.VMEM((heads, 1, rows), F32),
+            pltpu.VMEM((heads, VDIM, rows), F32),
+            dma((hops + 1,)),
+            dma((hops + 1,)),
+            dma((hops + 1, 4)),
+            dma((hops + 1, 4)),
+            dma((hops + 1, 2)),
+            dma((hops + 1, 2)),
+        ],
+        compiler_params=pltpu.CompilerParams(
+            collective_id=1, has_side_effects=True, vmem_limit_bytes=56 * 1024 * 1024
         ),
-        compiler_params=pltpu.CompilerParams(dimension_semantics=("arbitrary",)),
-    )(index.reshape(1), queries, gathered, w_key, w_value)
+    )(
+        query_latent, kv_latent, rotary_key.T, doc_ids[None, :],
+        query_gain, kv_gain, w_query_nope, w_query_rot.T, w_key, w_value,
+    )
 
 
 COLS = 512
@@ -140,7 +341,7 @@
 
 def mixer_kernel(
     chips,
-    att_ref, wout_ref, res_ref, gain_ref, meta_in, wg_hbm, wu_hbm, wd_hbm,
+    att_ref, wout_ref, res_ref, gain_ref, routes_ref, group_ref, logits_ref, wg_hbm, wu_hbm, wd_hbm,
     out_ref,
     wg_ref, wu_ref, wd_ref, part, relay_l, relay_r, sum_r, sum_l, from_l, from_r, mixed,
     meta, tok, sendb, rec, back_t, back_rl, back_rr, back_sr, back_sl, back_fl, back_fr, zb, gb,
@@ -183,6 +384,30 @@
     def cols_of(t):
         return pl.ds(pl.multiple_of(t * COLS, COLS), COLS)
 
+    routes = routes_ref[...]
+    expert = lax.broadcasted_iota(jnp.int32, (2 * chips, rows), 0)
+    goes = [routes[k : k + 1] == expert for k in range(2)]
+    earlier = (
+        lax.broadcasted_iota(jnp.int32, (rows, rows), 0)
+        < lax.broadcasted_iota(jnp.int32, (rows, rows), 1)
+    )
+    before = dot(
+        (goes[0] | goes[1]).astype(F32).astype(BF16), earlier.astype(F32).astype(BF16)
+    )
+    distance = lax.rem(lax.div(routes, 2) - z + chips, chips)
+    place = jnp.zeros_like(routes)
+    for p, offset in enumerate(offsets):
+        place = jnp.where(distance == offset % chips, p, place)
+    spot = (lax.rem(routes, 2) * (8 * chips) + place * 8 + core * 4).astype(F32)
+    ranks = [jnp.sum(jnp.where(g, before, 0.0), axis=0, keepdims=True) for g in goes]
+    logits = logits_ref[...]
+    top = jnp.maximum(logits[0:1], logits[1:2])
+    powers = [jnp.exp(logits[k : k + 1] - top) for k in range(2)]
+    share = group_ref[...][None, :] / (powers[0] + powers[1])
+    table = [spot[k : k + 1] + ranks[k] for k in range(2)] + [p * share for p in powers]
+    table.append(jnp.zeros((meta.shape[2] - 4, rows), F32))
+    meta[core] = jnp.concatenate(table, axis=0).T
+
     def project(t, carry):
         value = dot(att_ref[...], wout_ref[:, cols_of(t)])
         part[:, :, cols_of(t)] = value.reshape(4, rows, COLS).astype(BF16)
@@ -201,8 +426,7 @@
     pl.semaphore_wait(barrier, 3 + len(offsets) - 1)
     c_a = start(remote(part.at[across, :, lo], relay_l, ps.at[0], pr.at[0], to_right))
     c_d = start(remote(part.at[left, :, lo], from_r.at[:, lo], ps.at[1], pr.at[1], to_left))
-    meta[core] = meta_in[...]
-    m_x = start(remote(meta_in, meta.at[core], pair_s.at[0], pair_r.at[0], to_partner))
+    m_x = start(remote(meta.at[core], meta.at[core], pair_s.at[0], pair_r.at[0], to_partner))
     lax.fori_loop(tiles // 2, tiles, project, 0)
     c_b = start(remote(part.at[across, :, hi], relay_r, ps.at[2], pr.at[2], to_left))
     c_c = start(remote(part.at[right, :, hi], from_l.at[:, hi], ps.at[3], pr.at[3], to_right))
@@ -220,7 +444,7 @@
         + (part[x].astype(F32) + from_l[...].astype(F32) + from_r[...].astype(F32))
     ).astype(BF16)
     mixed[...] = after
-    tok[core] = norm_rows(after, gain_ref[...]).astype(BF16)
+    tok[core] = norm_rows(after, gain_ref[...][None, :]).astype(BF16)
     t_x = start(remote(tok.at[core], tok.at[core], pair_s.at[1], pair_r.at[1], to_partner))
     m_x.wait_recv()
     keys = meta[...].reshape(2 * rows, meta.shape[2])
@@ -282,8 +506,8 @@
             copy.wait_recv()
         many = 4 * SPAN * 8
         arrived = rec[:, q * SPAN : (q + 1) * SPAN].reshape(many, width)
-        gate = dot(arrived, wg_ref[...])
-        up = dot(arrived, wu_ref[...])
+        gate = dot_nt(arrived, wg_ref[...])
+        up = dot_nt(arrived, wu_ref[...])
         hidden = (gate / (1.0 + jnp.exp(-gate)) * up).astype(BF16)
 
         def down(t, carry):
@@ -360,7 +584,9 @@
         copy.wait_send()
 
 
-def mixer(attended, w_out, residual, gain, meta, w_gate, w_up, w_down, chips):
+def mixer(
+    attended, w_out, residual, gain, routes, group_weight, logits, w_gate, w_up, w_down, chips
+):
     rows, width = residual.shape
     n_chunks = chips // SPAN
     vmem = pl.BlockSpec(memory_space=pltpu.VMEM)
@@ -372,7 +598,7 @@
     return pl.pallas_call(
         functools.partial(mixer_kernel, chips),
         out_shape=jax.ShapeDtypeStruct((rows, width), BF16),
-        in_specs=[vmem] * 5 + [hbm] * 3,
+        in_specs=[vmem] * 7 + [hbm] * 3,
         out_specs=vmem,
         scratch_shapes=[
             pltpu.VMEM(w_gate.shape, BF16),
@@ -386,7 +612,7 @@
             pltpu.VMEM((rows, width), BF16),
             pltpu.VMEM((rows, width), BF16),
             pltpu.VMEM((rows, width), BF16),
-            pltpu.VMEM((2, rows, meta.shape[1]), F32),
+            pltpu.VMEM((2, rows, 128), F32),
             pltpu.VMEM((2, rows, width), BF16),
             pltpu.VMEM((chips, 8, width), BF16),
             pltpu.VMEM((4, chips, 8, width), BF16),
@@ -418,25 +644,7 @@
         compiler_params=pltpu.CompilerParams(
             collective_id=0, has_side_effects=True, vmem_limit_bytes=56 * 1024 * 1024
         ),
-    )(attended, w_out, residual, gain, meta, w_gate, w_up, w_down)
-
-
-def routing_meta(routes, group_weight, member_logits, chips):
-    sp = lax.axis_index("sp")
-    core, z = sp % 2, sp // 2
-    flat = routes.reshape(-1)
-    count = flat.shape[0]
-    earlier = jnp.arange(count)[None, :] < jnp.arange(count)[:, None]
-    same = flat[:, None] == flat[None, :]
-    ranking = jnp.sum((same & earlier).astype(jnp.int32), axis=1).reshape(routes.shape)
-    distance = (routes // 2 - z + chips) % chips
-    position = jnp.zeros_like(routes)
-    for p, offset in enumerate(offsets_of(chips)):
-        position = jnp.where(distance == offset % chips, p, position)
-    key = (routes % 2) * (8 * chips) + position * 8 + core * 4 + ranking
-    weights = group_weight[:, None] * jax.nn.softmax(member_logits, axis=-1)
-    filler = jnp.zeros((routes.shape[0], 124), F32)
-    return jnp.concatenate([key.astype(F32), weights, filler], axis=1)
+    )(attended, w_out, residual, gain, routes, group_weight, logits, w_gate, w_up, w_down)
 
 
 def on_device(
@@ -460,30 +668,14 @@
     group_weight,
     member_logits,
 ):
-    queries_here = query_latent.shape[0]
-    heads_here = w_key_nope.shape[1] // NOPE
-    index = lax.axis_index("sp")
     chips = lax.axis_size("sp") // 2
-    query_pos = index * queries_here + jnp.arange(queries_here, dtype=jnp.int32)
-    is_doc = doc_ids[:, None] == jnp.arange(ROPE, dtype=jnp.int32)[None, :]
-    key_normed = norm_rows(kv_latent, kv_gain).astype(BF16)
-    key_rot = rotate(rotary_key.astype(F32), query_pos).astype(BF16)
-    own = jnp.concatenate([key_normed, key_rot, is_doc.astype(BF16)], axis=1)
-    gathered = lax.all_gather(own, "sp", axis=0, tiled=True)
-
-    query_normed = norm_rows(query_latent, query_gain).astype(BF16)
-    query_nope = dot(query_normed, w_query_nope).astype(BF16)
-    query_nope = query_nope.reshape(queries_here, heads_here, NOPE)
-    query_rot = dot(query_normed, w_query_rot).reshape(queries_here, heads_here, ROPE)
-    query_rot = rotate(query_rot, query_pos).astype(BF16)
-    other_doc = jnp.where(is_doc, 0.0, FLOOR_SCORE).astype(BF16)
-    other_doc = jnp.broadcast_to(other_doc[:, None, :], query_rot.shape)
-    queries = jnp.concatenate([query_nope, query_rot, other_doc], axis=2).transpose(1, 0, 2)
-
-    attended = attention(index, queries, gathered, w_key_nope, w_value)
-    meta = routing_meta(routes, group_weight, member_logits, chips)
+    attended = attention(
+        query_latent, kv_latent, rotary_key, doc_ids, query_gain, kv_gain, w_query_nope,
+        w_query_rot, w_key_nope, w_value,
+    )
     return mixer(
-        attended, w_out, residual, ffn_gain[None, :], meta, w_gate[0], w_up[0], w_down[0], chips
+        attended, w_out, residual, ffn_gain, routes.T, group_weight, member_logits.T,
+        w_gate[0].T, w_up[0].T, w_down[0], chips,
     )
 
 

time: 275 us -> 190 us (0.69)
  waiting for transfers between devices: 83.4 us -> 0 us
  Pallas kernels: 162 us -> 188 us
  between operations: 13.7 us -> 0.02 us
  other arithmetic: 6.63 us -> 0 us
  local copies, waits for them, and re-layouts: 8.35 us -> 1.77 us
    all_gather x1 -> x0, waiting for transfers between devices: 83.3 us -> none  [on_device(): gathered = lax.all_gather(own, 'sp', axis=0, tiled=True)]
    pallas_call x1, Pallas kernels: 13.1 us -> 69.3 us  [attention(): pl.pallas_call(functools.partial(attention_kernel, (NOPE + ROPE) ** (-0.5...]
    pallas_call x1, Pallas kernels: 149 us -> 118 us  [mixer(): pl.pallas_call(functools.partial(mixer_kernel, chips), out_shape=jax.Shap...]
    unnamed x25 -> x1, local copies, waits for them, and re-layouts: 7.44 us -> 1.77 us
  transfers between devices with their start and end apart: 1 -> 0, of which waited for: 1 -> 0; matrix products, arithmetic and copies ran while one was open for 3% -> 0% of each run, Pallas kernels for 0% -> 0%
where the time goes in v2:
time: 190 us; the launch traced here: 189 us
  Pallas kernels  188 us (99%)
    pallas_call x1, Pallas kernels, mixer(): pl.pallas_call(functools.partial(mixer_kernel, chips), out_shape=jax.Shap...  118 us
    pallas_call x1, Pallas kernels, attention(): pl.pallas_call(functools.partial(attention_kernel, (NOPE + ROPE) ** (-0.5...  69.3 us

profile of v2, /device:TPU:33, one launch (start us, length us, event | category | flops | bytes accessed | tf_op | source)
XLA Modules:
  0.0 189.4 jit_solution(9143594012087937383)
XLA Ops:
  0.0 69.3 %shard_map.181.att_ref = bf16[256,384]{1,0:T(8,128)(2,1)} custom-call(bf16[256,768]{1,0:T(8,128)(2,1)} %ql_ref.1, bf16[256,384]{1,0:T(8,128)(2,1)} %kl_ref.1, bf16[64,256]{1,0:T(8,128)(2,1)} %bitcast.16, s32[1,256]{1,0:T(1,128)} %bitcast.17, f32[768]{0:T(1024)} %qg_ref.1, f32[384]{0:T(512)} %kg_ref.1, bf16[768,384]{1,0:T(8,128)(2,1)} %wqn_ref.1, ...), custom_call_target="tpu_custom_call" | custom-call | tf_op jit(solution)/shard_map/pallas_call | solution.py:301
  69.3 118.3 %shard_map.182 = bf16[64,3072]{1,0:T(8,128)(2,1)} custom-call(bf16[256,384]{1,0:T(8,128)(2,1)} %shard_map.181.att_ref, bf16[384,3072]{1,0:T(8,128)(2,1)} %wout_ref.1, bf16[64,3072]{1,0:T(8,128)(2,1)} %res_ref.1, f32[3072]{0:T(1024)} %gain_ref.1, s32[2,64]{1,0:T(2,128)} %bitcast.18, f32[64]{0:T(128)} %group_ref.1, f32[2,64]{1,0:T(2,128)} %bitcast.19, ...), custom_call_target="tpu_custom_call" | custom-call | tf_op jit(solution)/shard_map/pallas_call | solution.py:598
  187.6 1.8 copy.21

commit v3 on v2

--- a/solution.py
+++ b/solution.py
@@ -52,7 +52,9 @@
     to_right, to_left, to_partner = {"tp": right}, {"tp": left}, {"sp": sp + 1 - 2 * core}
 
     def chip_at(offset):
-        return {"sp": lax.rem(sp + 2 * offset + n_sp, n_sp)}
+        return {"sp": sp + 2 * offset}
+
+    chips = lax.div(n_sp, 2)
 
     rows = ql_ref.shape[0]
     heads = q_ref.shape[0]
@@ -60,9 +62,20 @@
     quarter = rows // 4
 
     barrier = pltpu.get_barrier_semaphore()
-    greeted = [to_partner, to_left, to_right] + [chip_at(o) for o in (1, -1, seed, -seed)]
-    for target in greeted:
+
+    def greet(target):
         pl.semaphore_signal(barrier, inc=1, device_id=target, device_id_type=MESH)
+
+    for target in (to_partner, to_left, to_right):
+        greet(target)
+    for offset in (1, seed):
+
+        @pl.when(z >= offset)
+        def _():
+            greet(chip_at(-offset))
+
+    has_next = z + 1 < chips
+    has_far = z + seed < chips
 
     def remote(src, dst, ssem, rsem, target):
         return pltpu.make_async_remote_copy(
@@ -116,9 +129,16 @@
     latent = norm_rows(kl_ref[...], kg_ref[...][None, :]).astype(BF16)
     own = jnp.concatenate([latent, key_tail], axis=1)
     kv[0, core] = own.reshape(4, quarter, own.shape[1])
-    pl.semaphore_wait(barrier, len(greeted))
-    onward(0).start()
-    jump().start()
+    pl.semaphore_wait(barrier, 3 + has_next.astype(jnp.int32) + has_far.astype(jnp.int32))
+
+    @pl.when(has_next)
+    def _():
+        onward(0).start()
+
+    @pl.when(has_far)
+    def _():
+        jump().start()
+
 
     def project(h):
         block = kv[h, core].reshape(rows, kv.shape[-1])
@@ -186,14 +206,24 @@
             l_ref[i] = total
             acc_ref[i] = attended
 
+    near, far = list(range(1, seed)), list(range(seed, hops + 1))
+    order = near[:3] + far[:1] + near[3:] + far[1:]
+
     def hop_at(n):
-        return jnp.where(n == hops, n, jnp.where(n % 2 == 1, (n + 1) // 2, seed - 1 + n // 2))
+        hop = n
+        for k, at in enumerate(order):
+            hop = jnp.where(n == k + 1, at, hop)
+        return hop
+
+    def exists(h):
+        return (h >= 1) & (h <= z) & ((h < hops) | ((h == hops) & (core == 1)))
+
+    def goes_on(h):
+        more = (h < hops - 1) | ((h == hops - 1) & (core == 1))
+        return (h != seed - 1) & more & has_next
 
     def held(n):
-        return (n >= 1) & ((n < hops) | ((n == hops) & (core == 1)))
-
-    def goes_on(h):
-        return (h != seed - 1) & ((h < hops - 1) | ((h == hops - 1) & (core == 1)))
+        return (n >= 1) & (n <= hops) & exists(hop_at(n))
 
     def arrive(n):
         @pl.when(held(n))
@@ -226,15 +256,13 @@
             project(h)
 
     def use(n):
-        @pl.when((n >= 1) & (n < hops))
+        h = hop_at(n)
+
+        @pl.when((n >= 1) & (n < hops) & (h <= z))
         def _():
-            h = hop_at(n)
             for copy in shared(h):
                 copy.wait_recv()
-
-            @pl.when(h <= z)
-            def _():
-                attend(h, (0, 1), False)
+            attend(h, (0, 1), False)
 
     arrive(1)
     for copy in shared(0):
@@ -250,25 +278,28 @@
 
     lax.fori_loop(2, hops + 3, tick, 0)
 
-    @pl.when(core == 0)
+    @pl.when((core == 0) & (hops <= z))
     def _():
         for copy in shared(hops):
             copy.wait_recv()
-
-        @pl.when(hops <= z)
-        def _():
-            attend(hops, (1,), False)
+        attend(hops, (1,), False)
 
     for i in range(heads):
         out_ref[:, i * VDIM : (i + 1) * VDIM] = (acc_ref[i] / l_ref[i]).T.astype(out_ref.dtype)
 
-    onward(0).wait_send()
-    jump().wait_send()
+    @pl.when(has_next)
+    def _():
+        onward(0).wait_send()
+
+    @pl.when(has_far)
+    def _():
+        jump().wait_send()
+
     for copy in shared(0):
         copy.wait_send()
 
     def drain(h, carry):
-        @pl.when(held(h))
+        @pl.when(exists(h))
         def _():
             @pl.when(goes_on(h))
             def _():
@@ -328,25 +359,27 @@
 
 
 COLS = 512
-SPAN = 4
+SPAN = 2
 
 
 def offsets_of(chips):
     half, quarter = chips // 2, chips // 4
-    offsets = [0, half, quarter, -quarter]
-    for m in range(1, quarter):
-        offsets += [m, -m, half - m, m - half]
+    offsets = [0, 1]
+    for m in range(1, quarter - 1):
+        offsets += [-m, m + 1]
+    for m in range(half, quarter - 1, -1):
+        offsets += [m, 1 - m]
     return offsets
 
 
 def mixer_kernel(
     chips,
-    att_ref, wout_ref, res_ref, gain_ref, routes_ref, group_ref, logits_ref, wg_hbm, wu_hbm, wd_hbm,
+    att_ref, res_ref, gain_ref, routes_ref, group_ref, logits_ref, wout_hbm, wg_hbm, wu_hbm, wd_hbm,
     out_ref,
-    wg_ref, wu_ref, wd_ref, part, relay_l, relay_r, sum_r, sum_l, from_l, from_r, mixed,
+    wout_ref, wg_ref, wu_ref, wd_ref, part, relay_l, relay_r, sum_r, sum_l, from_l, from_r, mixed,
     meta, tok, sendb, rec, back_t, back_rl, back_rr, back_sr, back_sl, back_fl, back_fr, zb, gb,
-    yb, yrecv,
-    wsem, pair_s, pair_r, ps, pr, zs, zr, xs, xr_, bs, br, gs, gr,
+    gb2,
+    wsem, pair_s, pair_r, hs, hr, ps, pr, zs, zr, xs, xr_, bs, br, gs, gr,
 ):
     sp = lax.axis_index("sp")
     x = lax.axis_index("tp")
@@ -367,6 +400,8 @@
     for target in [to_partner, to_left, to_right] + [on_ring(o) for o in offsets[1:]]:
         pl.semaphore_signal(barrier, inc=1, device_id=target, device_id_type=MESH)
 
+    w_load = pltpu.make_async_copy(wout_hbm, wout_ref, wsem.at[3])
+    w_load.start()
     loads = [
         pltpu.make_async_copy(wg_hbm, wg_ref, wsem.at[0]),
         pltpu.make_async_copy(wu_hbm, wu_ref, wsem.at[1]),
@@ -384,6 +419,28 @@
     def cols_of(t):
         return pl.ds(pl.multiple_of(t * COLS, COLS), COLS)
 
+    def project(t, carry):
+        value = dot(att_ref[...], wout_ref[:, cols_of(t)])
+        part[:, :, cols_of(t)] = value.reshape(4, rows, COLS).astype(BF16)
+        return carry
+
+    sends = []
+
+    def start(copy):
+        copy.start()
+        sends.append(copy)
+        return copy
+
+    lo, hi = pl.ds(0, half), pl.ds(half, half)
+    tiles = width // COLS
+    w_load.wait()
+    lax.fori_loop(0, tiles // 2, project, 0)
+    pl.semaphore_wait(barrier, 3 + len(offsets) - 1)
+    c_a = start(remote(part.at[across, :, lo], relay_l, ps.at[0], pr.at[0], to_right))
+    c_d = start(remote(part.at[left, :, lo], from_r.at[:, lo], ps.at[1], pr.at[1], to_left))
+    lax.fori_loop(tiles // 2, tiles, project, 0)
+    c_b = start(remote(part.at[across, :, hi], relay_r, ps.at[2], pr.at[2], to_left))
+    c_c = start(remote(part.at[right, :, hi], from_l.at[:, hi], ps.at[3], pr.at[3], to_right))
     routes = routes_ref[...]
     expert = lax.broadcasted_iota(jnp.int32, (2 * chips, rows), 0)
     goes = [routes[k : k + 1] == expert for k in range(2)]
@@ -408,28 +465,7 @@
     table.append(jnp.zeros((meta.shape[2] - 4, rows), F32))
     meta[core] = jnp.concatenate(table, axis=0).T
 
-    def project(t, carry):
-        value = dot(att_ref[...], wout_ref[:, cols_of(t)])
-        part[:, :, cols_of(t)] = value.reshape(4, rows, COLS).astype(BF16)
-        return carry
-
-    sends = []
-
-    def start(copy):
-        copy.start()
-        sends.append(copy)
-        return copy
-
-    lo, hi = pl.ds(0, half), pl.ds(half, half)
-    tiles = width // COLS
-    lax.fori_loop(0, tiles // 2, project, 0)
-    pl.semaphore_wait(barrier, 3 + len(offsets) - 1)
-    c_a = start(remote(part.at[across, :, lo], relay_l, ps.at[0], pr.at[0], to_right))
-    c_d = start(remote(part.at[left, :, lo], from_r.at[:, lo], ps.at[1], pr.at[1], to_left))
     m_x = start(remote(meta.at[core], meta.at[core], pair_s.at[0], pair_r.at[0], to_partner))
-    lax.fori_loop(tiles // 2, tiles, project, 0)
-    c_b = start(remote(part.at[across, :, hi], relay_r, ps.at[2], pr.at[2], to_left))
-    c_c = start(remote(part.at[right, :, hi], from_l.at[:, hi], ps.at[3], pr.at[3], to_right))
     c_a.wait_recv()
     sum_r[...] = (part[right, :, :half].astype(F32) + relay_l[...].astype(F32)).astype(BF16)
     c_e = start(remote(sum_r, from_l.at[:, lo], ps.at[4], pr.at[4], to_right))
@@ -563,23 +599,35 @@
             if 0 <= tick - s < n_chunks:
                 stages[s](tick - s)
 
-    for p in range(1, chips):
-        g_out[p].wait_recv()
-    weigh = jnp.where(first, keys[:, 2:3], 0.0) + jnp.where(second, keys[:, 3:4], 0.0)
-    weigh_hi = weigh.astype(BF16)
-    weigh_lo = (weigh - weigh_hi.astype(F32)).astype(BF16)
+    across_cores = []
+    for p in range(chips):
+        if p:
+            g_out[p].wait_recv()
+        across_cores.append(start(remote(gb.at[p], gb2.at[p], hs.at[p], hr.at[p], to_partner)))
+    mine = meta[core]
+
+    def weigh(parity):
+        here = (
+            lax.broadcasted_iota(jnp.int32, (rows, slots), 1) + parity * slots
+        ).astype(F32)
+        weight = jnp.where(mine[:, 0:1] == here, mine[:, 2:3], 0.0)
+        weight = weight + jnp.where(mine[:, 1:2] == here, mine[:, 3:4], 0.0)
+        high = weight.astype(BF16)
+        return high, (weight - high.astype(F32)).astype(BF16)
+
+    weights = [weigh(core), weigh(1 - core)]
+    for copy in across_cores:
+        copy.wait_recv()
 
     def combine(t, carry):
-        returned = gb[:, :, cols_of(t)].reshape(slots, COLS)
-        yb[:, :, cols_of(t)] = (dot(weigh_hi, returned) + dot(weigh_lo, returned)).reshape(
-            2, rows, COLS
-        )
+        routed = 0.0
+        for (high, low), blocks in zip(weights, (gb, gb2)):
+            returned = blocks[:, :, cols_of(t)].reshape(slots, COLS)
+            routed = routed + (dot(high, returned) + dot(low, returned))
+        out_ref[:, cols_of(t)] = (mixed[:, cols_of(t)].astype(F32) + routed).astype(out_ref.dtype)
         return carry
 
     lax.fori_loop(0, tiles, combine, 0)
-    y_x = start(remote(yb.at[1 - core], yrecv, pair_s.at[2], pair_r.at[2], to_partner))
-    y_x.wait_recv()
-    out_ref[...] = (mixed[...].astype(F32) + (yb[core] + yrecv[...])).astype(out_ref.dtype)
     for copy in sends:
         copy.wait_send()
 
@@ -598,9 +646,10 @@
     return pl.pallas_call(
         functools.partial(mixer_kernel, chips),
         out_shape=jax.ShapeDtypeStruct((rows, width), BF16),
-        in_specs=[vmem] * 7 + [hbm] * 3,
+        in_specs=[vmem] * 6 + [hbm] * 4,
         out_specs=vmem,
         scratch_shapes=[
+            pltpu.VMEM(w_out.shape, BF16),
             pltpu.VMEM(w_gate.shape, BF16),
             pltpu.VMEM(w_up.shape, BF16),
             pltpu.VMEM(w_down.shape, BF16),
@@ -625,11 +674,12 @@
             pltpu.VMEM(chunk, BF16),
             pltpu.VMEM(chunk, BF16),
             pltpu.VMEM((chips, 8, width), BF16),
-            pltpu.VMEM((2, rows, width), F32),
-            pltpu.VMEM((rows, width), F32),
-            dma((3,)),
-            dma((3,)),
-            dma((3,)),
+            pltpu.VMEM((chips, 8, width), BF16),
+            dma((4,)),
+            dma((2,)),
+            dma((2,)),
+            dma((chips,)),
+            dma((chips,)),
             dma((6,)),
             dma((6,)),
             dma((chips,)),
@@ -644,7 +694,7 @@
         compiler_params=pltpu.CompilerParams(
             collective_id=0, has_side_effects=True, vmem_limit_bytes=56 * 1024 * 1024
         ),
-    )(attended, w_out, residual, gain, routes, group_weight, logits, w_gate, w_up, w_down)
+    )(attended, residual, gain, routes, group_weight, logits, w_out, w_gate, w_up, w_down)
 
 
 def on_device(

time: 190 us -> 183 us (0.963)
  Pallas kernels: 188 us -> 181 us
    pallas_call x1, Pallas kernels: 69.3 us -> 28.1 us  [attention(): pl.pallas_call(functools.partial(attention_kernel, (NOPE + ROPE) ** (-0.5...]
    pallas_call x1, Pallas kernels: 118 us -> 153 us  [mixer(): pl.pallas_call(functools.partial(mixer_kernel, chips), out_shape=jax.Shap...]
where the time goes in v3:
time: 183 us
  Pallas kernels  181 us (99%)
    pallas_call x1, Pallas kernels, mixer(): pl.pallas_call(functools.partial(mixer_kernel, chips), out_shape=jax.Shap...  153 us
    pallas_call x1, Pallas kernels, attention(): pl.pallas_call(functools.partial(attention_kernel, (NOPE + ROPE) ** (-0.5...  28.1 us

profile of v3, /device:TPU:33, one launch (start us, length us, event | category | flops | bytes accessed | tf_op | source)
XLA Modules:
  0.0 182.5 jit_solution(10223346297077883666)
XLA Ops:
  0.0 28.1 %shard_map.181.att_ref = bf16[256,384]{1,0:T(8,128)(2,1)} custom-call(bf16[256,768]{1,0:T(8,128)(2,1)} %ql_ref.1, bf16[256,384]{1,0:T(8,128)(2,1)} %kl_ref.1, bf16[64,256]{1,0:T(8,128)(2,1)} %bitcast.16, s32[1,256]{1,0:T(1,128)} %bitcast.17, f32[768]{0:T(1024)} %qg_ref.1, f32[384]{0:T(512)} %kg_ref.1, bf16[768,384]{1,0:T(8,128)(2,1)} %wqn_ref.1, ...), custom_call_target="tpu_custom_call" | custom-call | tf_op jit(solution)/shard_map/pallas_call | solution.py:332
  28.1 152.6 %shard_map.182 = bf16[64,3072]{1,0:T(8,128)(2,1)} custom-call(bf16[256,384]{1,0:T(8,128)(2,1)} %shard_map.181.att_ref, bf16[64,3072]{1,0:T(8,128)(2,1)} %res_ref.1, f32[3072]{0:T(1024)} %gain_ref.1, s32[2,64]{1,0:T(2,128)} %bitcast.18, f32[64]{0:T(128)} %group_ref.1, f32[2,64]{1,0:T(2,128)} %bitcast.19, bf16[384,3072]{1,0:T(8,128)(2,1)} %wout_hbm.1, ...), custom_call_target="tpu_custom_call" | custom-call | tf_op jit(solution)/shard_map/pallas_call | solution.py:646
  180.8 1.8 copy.21

commit v4 on v3

--- a/solution.py
+++ b/solution.py
@@ -38,7 +38,7 @@
 
 
 def attention_kernel(
-    factor, hops, seed,
+    factor, hops,
     ql_ref, kl_ref, rk_ref, doc_ref, qg_ref, kg_ref, wqn_ref, wqr_ref, wk_ref, wv_ref,
     out_ref,
     kv, keys_ref, values_ref, q_ref, m_ref, l_ref, acc_ref, zs, zr, xs, xr_, ds, dr,
@@ -68,14 +68,12 @@
 
     for target in (to_partner, to_left, to_right):
         greet(target)
-    for offset in (1, seed):
-
-        @pl.when(z >= offset)
-        def _():
-            greet(chip_at(-offset))
+
+    @pl.when(z >= 1)
+    def _():
+        greet(chip_at(-1))
 
     has_next = z + 1 < chips
-    has_far = z + seed < chips
 
     def remote(src, dst, ssem, rsem, target):
         return pltpu.make_async_remote_copy(
@@ -83,14 +81,11 @@
             device_id_type=MESH,
         )
 
-    def onward(h):
+    def onward(h, k):
+        piece = pl.ds(k * (quarter // 2), quarter // 2)
         return remote(
-            kv.at[h, core, x], kv.at[h + 1, core, x], zs.at[h + 1], zr.at[h + 1], chip_at(1)
-        )
-
-    def jump():
-        return remote(
-            kv.at[0, core, x], kv.at[seed, core, x], zs.at[seed], zr.at[seed], chip_at(seed)
+            kv.at[h, core, x, piece], kv.at[h + 1, core, x, piece], zs.at[h + 1, k],
+            zr.at[h + 1, k], chip_at(1),
         )
 
     def beside(h, k):
@@ -129,15 +124,12 @@
     latent = norm_rows(kl_ref[...], kg_ref[...][None, :]).astype(BF16)
     own = jnp.concatenate([latent, key_tail], axis=1)
     kv[0, core] = own.reshape(4, quarter, own.shape[1])
-    pl.semaphore_wait(barrier, 3 + has_next.astype(jnp.int32) + has_far.astype(jnp.int32))
+    pl.semaphore_wait(barrier, 3 + has_next.astype(jnp.int32))
 
     @pl.when(has_next)
     def _():
-        onward(0).start()
-
-    @pl.when(has_far)
-    def _():
-        jump().start()
+        onward(0, 0).start()
+        onward(0, 1).start()
 
 
     def project(h):
@@ -206,59 +198,43 @@
             l_ref[i] = total
             acc_ref[i] = attended
 
-    near, far = list(range(1, seed)), list(range(seed, hops + 1))
-    order = near[:3] + far[:1] + near[3:] + far[1:]
-
-    def hop_at(n):
-        hop = n
-        for k, at in enumerate(order):
-            hop = jnp.where(n == k + 1, at, hop)
-        return hop
-
     def exists(h):
         return (h >= 1) & (h <= z) & ((h < hops) | ((h == hops) & (core == 1)))
 
     def goes_on(h):
         more = (h < hops - 1) | ((h == hops - 1) & (core == 1))
-        return (h != seed - 1) & more & has_next
-
-    def held(n):
-        return (n >= 1) & (n <= hops) & exists(hop_at(n))
-
-    def arrive(n):
-        @pl.when(held(n))
+        return more & has_next
+
+    def arrive(h):
+        @pl.when(exists(h))
         def _():
-            h = hop_at(n)
-            onward(h - 1).wait_recv()
-
-            @pl.when(goes_on(h))
-            def _():
-                onward(h).start()
+            for k in range(2):
+                onward(h - 1, k).wait_recv()
+
+                @pl.when(goes_on(h))
+                def _():
+                    onward(h, k).start()
 
             beside(h, 0).start()
             beside(h, 1).start()
 
-    def pass_on(n):
-        @pl.when(held(n))
+    def pass_on(h):
+        @pl.when(exists(h))
         def _():
-            h = hop_at(n)
             beside(h, 0).wait_recv()
             beside(h, 2).start()
             beside(h, 1).wait_recv()
             beside(h, 3).start()
 
-    def share(n):
-        @pl.when(held(n))
+    def share(h):
+        @pl.when(exists(h))
         def _():
-            h = hop_at(n)
             beside(h, 2).wait_recv()
             beside(h, 3).wait_recv()
             project(h)
 
-    def use(n):
-        h = hop_at(n)
-
-        @pl.when((n >= 1) & (n < hops) & (h <= z))
+    def use(h):
+        @pl.when((h >= 1) & (h < hops) & (h <= z))
         def _():
             for copy in shared(h):
                 copy.wait_recv()
@@ -272,11 +248,11 @@
     def tick(t, carry):
         arrive(t)
         pass_on(t - 1)
-        share(t - 2)
-        use(t - 3)
+        share(t - 3)
+        use(t - 4)
         return carry
 
-    lax.fori_loop(2, hops + 3, tick, 0)
+    lax.fori_loop(2, hops + 4, tick, 0)
 
     @pl.when((core == 0) & (hops <= z))
     def _():
@@ -289,11 +265,8 @@
 
     @pl.when(has_next)
     def _():
-        onward(0).wait_send()
-
-    @pl.when(has_far)
-    def _():
-        jump().wait_send()
+        onward(0, 0).wait_send()
+        onward(0, 1).wait_send()
 
     for copy in shared(0):
         copy.wait_send()
@@ -303,7 +276,8 @@
         def _():
             @pl.when(goes_on(h))
             def _():
-                onward(h).wait_send()
+                onward(h, 0).wait_send()
+                onward(h, 1).wait_send()
 
             for k in range(4):
                 beside(h, k).wait_send()
@@ -325,12 +299,11 @@
     latent_width = kv_latent.shape[1]
     blocks_back = (DOC_MOST + rows - 2) // rows
     hops = (blocks_back + 1) // 2
-    assert blocks_back % 2 == 1 and hops % 2 == 1
-    seed = (hops + 1) // 2
+    assert blocks_back % 2 == 1
     vmem = pl.BlockSpec(memory_space=pltpu.VMEM)
     dma = pltpu.SemaphoreType.DMA
     return pl.pallas_call(
-        functools.partial(attention_kernel, (NOPE + ROPE) ** (-0.5), hops, seed),
+        functools.partial(attention_kernel, (NOPE + ROPE) ** (-0.5), hops),
         out_shape=jax.ShapeDtypeStruct((rows, width), BF16),
         in_specs=[vmem] * 10,
         out_specs=vmem,
@@ -342,8 +315,8 @@
             pltpu.VMEM((heads, 1, rows), F32),
             pltpu.VMEM((heads, 1, rows), F32),
             pltpu.VMEM((heads, VDIM, rows), F32),
-            dma((hops + 1,)),
-            dma((hops + 1,)),
+            dma((hops + 1, 2)),
+            dma((hops + 1, 2)),
             dma((hops + 1, 4)),
             dma((hops + 1, 4)),
             dma((hops + 1, 2)),
@@ -367,9 +340,9 @@
     offsets = [0, 1]
     for m in range(1, quarter - 1):
         offsets += [-m, m + 1]
-    for m in range(half, quarter - 1, -1):
-        offsets += [m, 1 - m]
-    return offsets
+    for m in range(half - 1, quarter + 1, -1):
+        offsets += [m, -m]
+    return offsets[: half + 2] + [half, -quarter - 1, quarter + 1, -quarter, quarter, 1 - quarter]
 
 
 def mixer_kernel(
@@ -378,8 +351,8 @@
     out_ref,
     wout_ref, wg_ref, wu_ref, wd_ref, part, relay_l, relay_r, sum_r, sum_l, from_l, from_r, mixed,
     meta, tok, sendb, rec, back_t, back_rl, back_rr, back_sr, back_sl, back_fl, back_fr, zb, gb,
-    gb2,
-    wsem, pair_s, pair_r, hs, hr, ps, pr, zs, zr, xs, xr_, bs, br, gs, gr,
+    gb2, way, way_back,
+    wsem, wosem, ws, wr, pair_s, pair_r, hs, hr, ps, pr, zs, zr, xs, xr_, bs, br, gs, gr,
 ):
     sp = lax.axis_index("sp")
     x = lax.axis_index("tp")
@@ -400,15 +373,23 @@
     for target in [to_partner, to_left, to_right] + [on_ring(o) for o in offsets[1:]]:
         pl.semaphore_signal(barrier, inc=1, device_id=target, device_id_type=MESH)
 
-    w_load = pltpu.make_async_copy(wout_hbm, wout_ref, wsem.at[3])
-    w_load.start()
+    tiles = width // COLS
+
+    def cols_of(t):
+        return pl.ds(pl.multiple_of(t * COLS, COLS), COLS)
+
+    def w_load(t):
+        return pltpu.make_async_copy(
+            wout_hbm.at[:, cols_of(t)], wout_ref.at[:, cols_of(t)], wosem.at[t]
+        )
+
+    for t in range(tiles):
+        w_load(t).start()
     loads = [
         pltpu.make_async_copy(wg_hbm, wg_ref, wsem.at[0]),
         pltpu.make_async_copy(wu_hbm, wu_ref, wsem.at[1]),
         pltpu.make_async_copy(wd_hbm, wd_ref, wsem.at[2]),
     ]
-    for load in loads:
-        load.start()
 
     def remote(src, dst, ssem, rsem, target):
         return pltpu.make_async_remote_copy(
@@ -416,10 +397,8 @@
             device_id_type=MESH,
         )
 
-    def cols_of(t):
-        return pl.ds(pl.multiple_of(t * COLS, COLS), COLS)
-
     def project(t, carry):
+        w_load(t).wait()
         value = dot(att_ref[...], wout_ref[:, cols_of(t)])
         part[:, :, cols_of(t)] = value.reshape(4, rows, COLS).astype(BF16)
         return carry
@@ -432,13 +411,13 @@
         return copy
 
     lo, hi = pl.ds(0, half), pl.ds(half, half)
-    tiles = width // COLS
-    w_load.wait()
     lax.fori_loop(0, tiles // 2, project, 0)
     pl.semaphore_wait(barrier, 3 + len(offsets) - 1)
     c_a = start(remote(part.at[across, :, lo], relay_l, ps.at[0], pr.at[0], to_right))
     c_d = start(remote(part.at[left, :, lo], from_r.at[:, lo], ps.at[1], pr.at[1], to_left))
     lax.fori_loop(tiles // 2, tiles, project, 0)
+    for load in loads:
+        load.start()
     c_b = start(remote(part.at[across, :, hi], relay_r, ps.at[2], pr.at[2], to_left))
     c_c = start(remote(part.at[right, :, hi], from_l.at[:, hi], ps.at[3], pr.at[3], to_right))
     routes = routes_ref[...]
@@ -499,14 +478,48 @@
         sendb[:, :, cols_of(t)] = picked.reshape(chips, 8, COLS).astype(BF16)
         return carry
 
+    opposite = offsets.index(chips // 2)
+    quarter = chips // 4
+
+    def both_ways(block, buffers, first, ssems, rsems):
+        return [
+            start(
+                remote(
+                    block.at[:, cols], buffers.at[k], ssems.at[first + k], rsems.at[first + k],
+                    on_ring(side * quarter),
+                )
+            )
+            for k, (cols, side) in enumerate(((lo, 1), (hi, -1)))
+        ]
+
+    def hand_on(arriving, buffers, block):
+        base = 0 if buffers is way else 4
+        for k, (cols, side) in enumerate(((lo, 1), (hi, -1))):
+            arriving[k].wait_recv()
+            arriving.append(
+                start(
+                    remote(
+                        buffers.at[k], block.at[:, cols], ws.at[base + 2 + k],
+                        wr.at[base + 2 + k], on_ring(side * quarter),
+                    )
+                )
+            )
+
+    def arrived_in_full(copies):
+        for copy in copies[2:] if isinstance(copies, list) else [copies]:
+            copy.wait_recv()
+
     lax.fori_loop(0, tiles, select, 0)
     z_out = [None]
-    for p in range(1, chips):
-        z_out.append(
-            start(
+    z_out += [None] * (chips - 1)
+    near = list(range(1, 6))
+    for p in near + [opposite] + [p for p in range(6, chips) if p != opposite]:
+        if p == opposite:
+            z_out[p] = both_ways(sendb.at[p], way, 0, ws, wr)
+        else:
+            z_out[p] = start(
                 remote(sendb.at[p], rec.at[x, p], zs.at[p], zr.at[p], on_ring(offsets[p]))
             )
-        )
     rec[x, 0] = sendb[0]
     for load in loads:
         load.wait()
@@ -516,7 +529,7 @@
     def spread(q):
         for p in range(q * SPAN, (q + 1) * SPAN):
             if p:
-                z_out[p].wait_recv()
+                arrived_in_full(z_out[p])
         whole = pl.ds(q * SPAN, SPAN)
         fwd[q] = [
             start(remote(rec.at[x, whole], rec.at[x, whole], xs.at[q, 0], xr_.at[q, 0], to_right)),
@@ -586,23 +599,30 @@
         ).astype(BF16)
         for k in range(SPAN):
             p = q * SPAN + k
-            if p:
+            if p == opposite:
+                g_out[p] = both_ways(zb.at[q, k], way_back, 4, ws, wr)
+            elif p:
                 g_out[p] = start(
                     remote(zb.at[q, k], gb.at[p], gs.at[p], gr.at[p], on_ring(-offsets[p]))
                 )
             else:
                 gb[0] = zb[0, 0]
 
-    stages = (spread, relay, experts, add_relayed, give_back)
-    for tick in range(n_chunks + len(stages) - 1):
-        for s in reversed(range(len(stages))):
-            if 0 <= tick - s < n_chunks:
-                stages[s](tick - s)
+    stages = ((give_back, 4), (add_relayed, 3), (experts, 2), (relay, 1), (spread, 0))
+    opposite_chunk = opposite // SPAN
+    for tick in range(n_chunks + 4):
+        if tick == 2:
+            hand_on(z_out[opposite], way, rec.at[x, opposite])
+        if tick == opposite_chunk + 5:
+            hand_on(g_out[opposite], way_back, gb.at[opposite])
+        for stage, lag in stages:
+            if 0 <= tick - lag < n_chunks:
+                stage(tick - lag)
 
     across_cores = []
     for p in range(chips):
         if p:
-            g_out[p].wait_recv()
+            arrived_in_full(g_out[p])
         across_cores.append(start(remote(gb.at[p], gb2.at[p], hs.at[p], hr.at[p], to_partner)))
     mine = meta[core]
 
@@ -675,7 +695,12 @@
             pltpu.VMEM(chunk, BF16),
             pltpu.VMEM((chips, 8, width), BF16),
             pltpu.VMEM((chips, 8, width), BF16),
-            dma((4,)),
+            pltpu.VMEM((2, 8, half), BF16),
+            pltpu.VMEM((2, 8, half), BF16),
+            dma((3,)),
+            dma((width // COLS,)),
+            dma((8,)),
+            dma((8,)),
             dma((2,)),
             dma((2,)),
             dma((chips,)),

time: 183 us -> 174 us (0.951)
  Pallas kernels: 181 us -> 172 us
    pallas_call x1, Pallas kernels: 153 us -> 144 us  [mixer(): pl.pallas_call(functools.partial(mixer_kernel, chips), out_shape=jax.Shap...]
where the time goes in v4:
time: 174 us
  Pallas kernels  172 us (99%)
  local copies, waits for them, and re-layouts  1.77 us (1%)
    pallas_call x1, Pallas kernels, mixer(): pl.pallas_call(functools.partial(mixer_kernel, chips), out_shape=jax.Shap...  144 us
    pallas_call x1, Pallas kernels, attention(): pl.pallas_call(functools.partial(attention_kernel, (NOPE + ROPE) ** (-0.5...  28.2 us

profile of v4, /device:TPU:33, one launch (start us, length us, event | category | flops | bytes accessed | tf_op | source)
XLA Modules:
  0.0 174.1 jit_solution(17648600124177535425)
XLA Ops:
  0.0 28.2 %shard_map.181.att_ref = bf16[256,384]{1,0:T(8,128)(2,1)} custom-call(bf16[256,768]{1,0:T(8,128)(2,1)} %ql_ref.1, bf16[256,384]{1,0:T(8,128)(2,1)} %kl_ref.1, bf16[64,256]{1,0:T(8,128)(2,1)} %bitcast.16, s32[1,256]{1,0:T(1,128)} %bitcast.17, f32[768]{0:T(1024)} %qg_ref.1, f32[384]{0:T(512)} %kg_ref.1, bf16[768,384]{1,0:T(8,128)(2,1)} %wqn_ref.1, ...), custom_call_target="tpu_custom_call" | custom-call | tf_op jit(solution)/shard_map/pallas_call | solution.py:305
  28.2 144.1 %shard_map.182 = bf16[64,3072]{1,0:T(8,128)(2,1)} custom-call(bf16[256,384]{1,0:T(8,128)(2,1)} %shard_map.181.att_ref, bf16[64,3072]{1,0:T(8,128)(2,1)} %res_ref.1, f32[3072]{0:T(1024)} %gain_ref.1, s32[2,64]{1,0:T(2,128)} %bitcast.18, f32[64]{0:T(128)} %group_ref.1, f32[2,64]{1,0:T(2,128)} %bitcast.19, bf16[384,3072]{1,0:T(8,128)(2,1)} %wout_hbm.1, ...), custom_call_target="tpu_custom_call" | custom-call | tf_op jit(solution)/shard_map/pallas_call | solution.py:666
  172.3 1.8 %copy.21 = bf16[64,3072]{1,0:T(8,128)(2,1)} copy(bf16[64,3072]{1,0:T(8,128)(2,1)} %shard_map.182) | data formatting | bytes 786432

commit v5 on v4

--- a/solution.py
+++ b/solution.py
@@ -337,12 +337,13 @@
 
 def offsets_of(chips):
     half, quarter = chips // 2, chips // 4
-    offsets = [0, 1]
-    for m in range(1, quarter - 1):
-        offsets += [-m, m + 1]
-    for m in range(half - 1, quarter + 1, -1):
+    offsets = [0, 1, -2, 3]
+    for m in range(half - 1, quarter, -1):
         offsets += [m, -m]
-    return offsets[: half + 2] + [half, -quarter - 1, quarter + 1, -quarter, quarter, 1 - quarter]
+    offsets += [half, -quarter]
+    for m in range(quarter, 3, -1):
+        offsets += [m, 1 - m]
+    return offsets + [2, -1]
 
 
 def mixer_kernel(
@@ -351,8 +352,8 @@
     out_ref,
     wout_ref, wg_ref, wu_ref, wd_ref, part, relay_l, relay_r, sum_r, sum_l, from_l, from_r, mixed,
     meta, tok, sendb, rec, back_t, back_rl, back_rr, back_sr, back_sl, back_fl, back_fr, zb, gb,
-    gb2, way, way_back,
-    wsem, wosem, ws, wr, pair_s, pair_r, hs, hr, ps, pr, zs, zr, xs, xr_, bs, br, gs, gr,
+    gb2, way, way_back, outb,
+    wsem, wosem, osem, ws, wr, pair_s, pair_r, hs, hr, ps, pr, zs, zr, xs, xr_, bs, br, gs, gr,
 ):
     sp = lax.axis_index("sp")
     x = lax.axis_index("tp")
@@ -512,14 +513,16 @@
     lax.fori_loop(0, tiles, select, 0)
     z_out = [None]
     z_out += [None] * (chips - 1)
-    near = list(range(1, 6))
-    for p in near + [opposite] + [p for p in range(6, chips) if p != opposite]:
-        if p == opposite:
-            z_out[p] = both_ways(sendb.at[p], way, 0, ws, wr)
-        else:
+
+    def send_blocks(positions):
+        for p in positions:
             z_out[p] = start(
                 remote(sendb.at[p], rec.at[x, p], zs.at[p], zr.at[p], on_ring(offsets[p]))
             )
+
+    send_blocks(range(1, SPAN * 2))
+    z_out[opposite] = both_ways(sendb.at[opposite], way, 0, ws, wr)
+    send_blocks(range(SPAN * 2, opposite))
     rec[x, 0] = sendb[0]
     for load in loads:
         load.wait()
@@ -613,6 +616,7 @@
     for tick in range(n_chunks + 4):
         if tick == 2:
             hand_on(z_out[opposite], way, rec.at[x, opposite])
+            send_blocks(range(opposite + 1, chips))
         if tick == opposite_chunk + 5:
             hand_on(g_out[opposite], way_back, gb.at[opposite])
         for stage, lag in stages:
@@ -644,10 +648,18 @@
         for (high, low), blocks in zip(weights, (gb, gb2)):
             returned = blocks[:, :, cols_of(t)].reshape(slots, COLS)
             routed = routed + (dot(high, returned) + dot(low, returned))
-        out_ref[:, cols_of(t)] = (mixed[:, cols_of(t)].astype(F32) + routed).astype(out_ref.dtype)
+        outb[:, cols_of(t)] = (mixed[:, cols_of(t)].astype(F32) + routed).astype(outb.dtype)
+        put_out(t).start()
         return carry
 
+    def put_out(t):
+        return pltpu.make_async_copy(
+            outb.at[:, cols_of(t)], out_ref.at[:, cols_of(t)], osem.at[t]
+        )
+
     lax.fori_loop(0, tiles, combine, 0)
+    for t in range(tiles):
+        put_out(t).wait()
     for copy in sends:
         copy.wait_send()
 
@@ -667,7 +679,7 @@
         functools.partial(mixer_kernel, chips),
         out_shape=jax.ShapeDtypeStruct((rows, width), BF16),
         in_specs=[vmem] * 6 + [hbm] * 4,
-        out_specs=vmem,
+        out_specs=hbm,
         scratch_shapes=[
             pltpu.VMEM(w_out.shape, BF16),
             pltpu.VMEM(w_gate.shape, BF16),
@@ -697,7 +709,9 @@
             pltpu.VMEM((chips, 8, width), BF16),
             pltpu.VMEM((2, 8, half), BF16),
             pltpu.VMEM((2, 8, half), BF16),
+            pltpu.VMEM((rows, width), BF16),
             dma((3,)),
+            dma((width // COLS,)),
             dma((width // COLS,)),
             dma((8,)),
             dma((8,)),

time: 174 us -> 170 us (0.977)
  Pallas kernels: 172 us -> 168 us
    pallas_call x1, Pallas kernels: 144 us -> 139 us  [mixer(): pl.pallas_call(functools.partial(mixer_kernel, chips), out_shape=jax.Shap...]
where the time goes in v5:
time: 170 us; the launch traced here: 169 us
  Pallas kernels  168 us (99%)
  local copies, waits for them, and re-layouts  1.77 us (1%)
    pallas_call x1, Pallas kernels, mixer(): pl.pallas_call(functools.partial(mixer_kernel, chips), out_shape=jax.Shap...  139 us
    pallas_call x1, Pallas kernels, attention(): pl.pallas_call(functools.partial(attention_kernel, (NOPE + ROPE) ** (-0.5...  28.2 us

profile of v5, /device:TPU:33, one launch (start us, length us, event | category | flops | bytes accessed | tf_op | source)
XLA Modules:
  0.0 169.3 jit_solution(8970354741012902354)
XLA Ops:
  0.0 28.2 %shard_map.181.att_ref = bf16[256,384]{1,0:T(8,128)(2,1)} custom-call(bf16[256,768]{1,0:T(8,128)(2,1)} %ql_ref.1, bf16[256,384]{1,0:T(8,128)(2,1)} %kl_ref.1, bf16[64,256]{1,0:T(8,128)(2,1)} %bitcast.16, s32[1,256]{1,0:T(1,128)} %bitcast.17, f32[768]{0:T(1024)} %qg_ref.1, f32[384]{0:T(512)} %kg_ref.1, bf16[768,384]{1,0:T(8,128)(2,1)} %wqn_ref.1, ...), custom_call_target="tpu_custom_call" | custom-call | tf_op jit(solution)/shard_map/pallas_call | solution.py:305
  28.2 139.4 %shard_map.182 = bf16[64,3072]{1,0:T(8,128)(2,1)} custom-call(bf16[256,384]{1,0:T(8,128)(2,1)} %shard_map.181.att_ref, bf16[64,3072]{1,0:T(8,128)(2,1)} %res_ref.1, f32[3072]{0:T(1024)} %gain_ref.1, s32[2,64]{1,0:T(2,128)} %bitcast.18, f32[64]{0:T(128)} %group_ref.1, f32[2,64]{1,0:T(2,128)} %bitcast.19, bf16[384,3072]{1,0:T(8,128)(2,1)} %wout_hbm.1, ...), custom_call_target="tpu_custom_call" | custom-call | tf_op jit(solution)/shard_map/pallas_call | solution.py:678
  167.5 1.8 %copy.21 = bf16[64,3072]{1,0:T(8,128)(2,1)} copy(bf16[64,3072]{1,0:T(8,128)(2,1)} %shard_map.182) | data formatting | bytes 786432

commit v6 on v5

--- a/solution.py
+++ b/solution.py
@@ -350,7 +350,7 @@
     chips,
     att_ref, res_ref, gain_ref, routes_ref, group_ref, logits_ref, wout_hbm, wg_hbm, wu_hbm, wd_hbm,
     out_ref,
-    wout_ref, wg_ref, wu_ref, wd_ref, part, relay_l, relay_r, sum_r, sum_l, from_l, from_r, mixed,
+    wout_ref, wg_ref, wu_ref, wd_ref, wgt_ref, wut_ref, part, relay_l, relay_r, sum_r, sum_l, from_l, from_r, mixed,
     meta, tok, sendb, rec, back_t, back_rl, back_rr, back_sr, back_sl, back_fl, back_fr, zb, gb,
     gb2, way, way_back, outb,
     wsem, wosem, osem, ws, wr, pair_s, pair_r, hs, hr, ps, pr, zs, zr, xs, xr_, bs, br, gs, gr,
@@ -452,6 +452,15 @@
     c_b.wait_recv()
     sum_l[...] = (part[left, :, half:].astype(F32) + relay_r[...].astype(F32)).astype(BF16)
     c_f = start(remote(sum_l, from_r.at[:, hi], ps.at[5], pr.at[5], to_left))
+    for load in loads:
+        load.wait()
+
+    def turn(t, carry):
+        wgt_ref[cols_of(t), :] = wg_ref[:, cols_of(t)].T
+        wut_ref[cols_of(t), :] = wu_ref[:, cols_of(t)].T
+        return carry
+
+    lax.fori_loop(0, tiles, turn, 0)
     for copy in (c_d, c_c, c_e, c_f):
         copy.wait_recv()
 
@@ -524,8 +533,6 @@
     z_out[opposite] = both_ways(sendb.at[opposite], way, 0, ws, wr)
     send_blocks(range(SPAN * 2, opposite))
     rec[x, 0] = sendb[0]
-    for load in loads:
-        load.wait()
 
     fwd = [None] * n_chunks
 
@@ -558,8 +565,8 @@
             copy.wait_recv()
         many = 4 * SPAN * 8
         arrived = rec[:, q * SPAN : (q + 1) * SPAN].reshape(many, width)
-        gate = dot_nt(arrived, wg_ref[...])
-        up = dot_nt(arrived, wu_ref[...])
+        gate = dot(arrived, wgt_ref[...])
+        up = dot(arrived, wut_ref[...])
         hidden = (gate / (1.0 + jnp.exp(-gate)) * up).astype(BF16)
 
         def down(t, carry):
@@ -685,6 +692,8 @@
             pltpu.VMEM(w_gate.shape, BF16),
             pltpu.VMEM(w_up.shape, BF16),
             pltpu.VMEM(w_down.shape, BF16),
+            pltpu.VMEM(w_gate.shape[::-1], BF16),
+            pltpu.VMEM(w_up.shape[::-1], BF16),
             pltpu.VMEM((4, rows, width), BF16),
             pltpu.VMEM((rows, half), BF16),
             pltpu.VMEM((rows, half), BF16),

time: 170 us -> 170 us (level)
  no operation moved by 1% of the time
where the time goes in v6:
time: 170 us
  Pallas kernels  168 us (99%)
  local copies, waits for them, and re-layouts  1.77 us (1%)
    pallas_call x1, Pallas kernels, mixer(): pl.pallas_call(functools.partial(mixer_kernel, chips), out_shape=jax.Shap...  140 us
    pallas_call x1, Pallas kernels, attention(): pl.pallas_call(functools.partial(attention_kernel, (NOPE + ROPE) ** (-0.5...  28.2 us

profile of v6, /device:TPU:33, one launch (start us, length us, event | category | flops | bytes accessed | tf_op | source)
XLA Modules:
  0.0 169.9 jit_solution(18309421619372046230)
XLA Ops:
  0.0 28.2 %shard_map.181.att_ref = bf16[256,384]{1,0:T(8,128)(2,1)} custom-call(bf16[256,768]{1,0:T(8,128)(2,1)} %ql_ref.1, bf16[256,384]{1,0:T(8,128)(2,1)} %kl_ref.1, bf16[64,256]{1,0:T(8,128)(2,1)} %bitcast.16, s32[1,256]{1,0:T(1,128)} %bitcast.17, f32[768]{0:T(1024)} %qg_ref.1, f32[384]{0:T(512)} %kg_ref.1, bf16[768,384]{1,0:T(8,128)(2,1)} %wqn_ref.1, ...), custom_call_target="tpu_custom_call" | custom-call | tf_op jit(solution)/shard_map/pallas_call | solution.py:305
  28.2 140.0 %shard_map.182 = bf16[64,3072]{1,0:T(8,128)(2,1)} custom-call(bf16[256,384]{1,0:T(8,128)(2,1)} %shard_map.181.att_ref, bf16[64,3072]{1,0:T(8,128)(2,1)} %res_ref.1, f32[3072]{0:T(1024)} %gain_ref.1, s32[2,64]{1,0:T(2,128)} %bitcast.18, f32[64]{0:T(128)} %group_ref.1, f32[2,64]{1,0:T(2,128)} %bitcast.19, bf16[384,3072]{1,0:T(8,128)(2,1)} %wout_hbm.1, ...), custom_call_target="tpu_custom_call" | custom-call | tf_op jit(solution)/shard_map/pallas_call | solution.py:685
  168.1 1.8 %copy.21 = bf16[64,3072]{1,0:T(8,128)(2,1)} copy(bf16[64,3072]{1,0:T(8,128)(2,1)} %shard_map.182) | data formatting | bytes 786432
